TPU v7x, 32 devices: a whole 2x2x4 slice. The times are simulated.
32 devices in a mesh: ep: 4 (over y, x), tp: 8 (over z, core).
Axes of the slice: x: 2, y: 2, z: 4, core: 2. Of those that a mesh axis runs over, the one named last changes fastest.
Arguments:
- pool_in: bfloat16 [16384, 1024], P(('ep', 'tp')), may hold values from -6 to 6
- pool_weight: bfloat16 [4, 256, 256], replicated, may hold values from -0.375 to 0.375
- pool_gain: float32 [1024], replicated, may hold values from 0.1 to 1.9
- out_weight: bfloat16 [1024, 2048], P('tp'), may hold values from -0.1875 to 0.1875
- mix_gain: float32 [2048], replicated, may hold values from 0.1 to 1.9
- expert_in: bfloat16 [1024, 2048], P('ep'), may hold values from -6 to 6
- routes: int32 [1024, 4], P('ep'), may hold values from 0 to 7, all different within a row; in each aligned block of 32 rows (0 to 31, 32 to 63, ...) at most 32 rows name the same one
- route_weight: float32 [1024, 4], P('ep'), may hold values from 0.1 to 1
- pre_gain: float32 [2048], replicated, may hold values from 0.1 to 1.9
- gate_weight: bfloat16 [8, 2048, 4096], P('ep', None, 'tp'), may hold values from -0.39648438 to 0.39648438
- up_weight: bfloat16 [8, 2048, 4096], P('ep', None, 'tp'), may hold values from -0.39648438 to 0.39648438
- down_weight: bfloat16 [8, 4096, 2048], P('ep', 'tp'), may hold values from -0.09375 to 0.09375
- post_gain: float32 [2048], replicated, may hold values from 0.1 to 1.9
Outputs:
- mix_out: bfloat16 [16384, 2048], P(('ep', 'tp'))
- expert_out: bfloat16 [1024, 2048], P(('ep', 'tp'))
Inputs may be any that keep to these rules, and one draw needn't show every extreme that they name: `routes`: each row names 4 different experts. In each aligned block of 32 rows no expert is named by more than 32 rows, a bound that some block reaches.
All inputs are finite; a program needn't handle non-finite values.
Results may differ from a plain program's by a relative error of at most 0.019.
Values may be sent and summed in bfloat16 or wider, within the bound.
A program may use at most 128 MiB of HBM per device.

v0:
```python
import functools

import jax
import jax.numpy as jnp
from jax import lax
from jax.experimental import pallas as pl
from jax.experimental.pallas import tpu as pltpu
from jax.sharding import PartitionSpec as P

WINDOWS = (2, 4, 8, 16)
EPS = 1e-06
LIMIT = 7.0
ALPHA = 1.702
LANES = 128
TILE = 512
POOL_ROWS = 128
PROJECT_ROWS = 256
MESH = pl.DeviceIdType.MESH


def rms_scale(values, gain):
    mean_square = jnp.mean(values * values, axis=-1, keepdims=True)
    return values * lax.rsqrt(mean_square + EPS) * gain


def expert_weights(routes, route_weight, experts):
    chosen = routes[:, :, None] == jnp.arange(experts, dtype=jnp.int32)[None, None, :]
    return jnp.sum(jnp.where(chosen, route_weight[:, :, None], 0.0), axis=1)


def clamped_unit(gate, up):
    gate = jnp.minimum(gate, LIMIT)
    up = jnp.clip(up, -LIMIT, LIMIT)
    return (up + 1.0) * gate * jax.nn.sigmoid(ALPHA * gate)


def flipped(place, mask, count):
    result, bit = 0, 1
    while bit < count:
        result = result + ((place // bit + mask // bit) % 2) * bit
        bit *= 2
    return result


def expert_kernel(
    n_ep,
    n_tp,
    expert_in_ref,
    packed_ref,
    pre_gain_ref,
    gate_hbm,
    up_hbm,
    down_hbm,
    gain_ref,
    pool_ref,
    pool_weight_ref,
    pool_gain_ref,
    out_weight_ref,
    mix_gain_ref,
    mix_ref,
    out_ref,
    own_ref,
    rim_ref,
    padded_ref,
    mixed_ref,
    all_weight_ref,
    x_ref,
    gate_ref,
    up_ref,
    down_ref,
    hid_ref,
    part_ref,
    core_ref,
    peer_ref,
    acc_ref,
    zsend_ref,
    zrecv_ref,
    load_sem,
    ag_send,
    ag_recv,
    fw_send,
    fw_recv,
    cs_send,
    cs_recv,
    ep_send,
    ep_recv,
    z_send,
    z_recv,
    rim_send,
    rim_recv,
    w_send,
    w_recv,
    wf_send,
    wf_recv,
):
    ep, tp = lax.axis_index("ep"), lax.axis_index("tp")
    core, z = tp % 2, tp // 2
    partner = z * 2 + 1 - core
    n_z = n_tp // 2
    tokens = own_ref.shape[0]
    experts, width, units = gate_ref.shape
    tiles = width // TILE
    half = pl.ds(pl.multiple_of(core * (tokens // 2), tokens // 2), tokens // 2)
    last = n_ep - 1

    loads = [
        pltpu.make_async_copy(gate_hbm, gate_ref, load_sem.at[0]),
        pltpu.make_async_copy(up_hbm, up_ref, load_sem.at[1]),
        pltpu.make_async_copy(down_hbm, down_ref, load_sem.at[2]),
    ]
    for load in loads:
        load.start()

    def ep_peer(k):
        return {"ep": flipped(ep, k + 1, n_ep)}

    def z_peer(k):
        return flipped(z, k + 1, n_z)

    place = ep * n_tp + tp
    devices = n_ep * n_tp
    after, before = (place + 1) % devices, (place + devices - 1) % devices

    def at(device):
        return {"ep": device // n_tp, "tp": device % n_tp}

    barrier = pltpu.get_barrier_semaphore()
    pl.semaphore_signal(barrier, inc=1, device_id=at(after), device_id_type=MESH)
    pl.semaphore_signal(barrier, inc=1, device_id=at(before), device_id_type=MESH)
    pl.semaphore_signal(barrier, inc=1, device_id={"tp": partner}, device_id_type=MESH)
    for k in range(n_ep - 1):
        pl.semaphore_signal(barrier, inc=1, device_id=ep_peer(k), device_id_type=MESH)
    for k in range(n_z - 1):
        pl.semaphore_signal(
            barrier, inc=1, device_id={"tp": z_peer(k) * 2 + core}, device_id_type=MESH
        )
    own_ref[:, :width] = rms_scale(
        expert_in_ref[...].astype(jnp.float32), pre_gain_ref[...]
    ).astype(jnp.bfloat16)
    own_ref[:, width:] = packed_ref[...]
    pl.semaphore_wait(barrier, n_ep + n_z + 1)

    def gather_copy(k):
        return pltpu.make_async_remote_copy(
            own_ref.at[half],
            x_ref.at[k, half],
            ag_send.at[k],
            ag_recv.at[k],
            device_id=ep_peer(k),
            device_id_type=MESH,
        )

    def forward_copy(k):
        return pltpu.make_async_remote_copy(
            x_ref.at[k, half],
            x_ref.at[k, half],
            fw_send.at[k],
            fw_recv.at[k],
            device_id={"tp": partner},
            device_id_type=MESH,
        )

    def core_copy(k, j):
        return pltpu.make_async_remote_copy(
            part_ref.at[j, :, 1 - core],
            core_ref.at[k, j],
            cs_send.at[j],
            cs_recv.at[k, j],
            device_id={"tp": partner},
            device_id_type=MESH,
        )

    def peer_copy(k):
        return pltpu.make_async_remote_copy(
            core_ref.at[k],
            peer_ref.at[k],
            ep_send.at[k],
            ep_recv.at[k],
            device_id=ep_peer(k),
            device_id_type=MESH,
        )

    def z_copy(k):
        return pltpu.make_async_remote_copy(
            zsend_ref.at[z_peer(k)],
            zrecv_ref.at[k],
            z_send.at[k],
            z_recv.at[k],
            device_id={"tp": z_peer(k) * 2 + core},
            device_id_type=MESH,
        )

    rows, channels = pool_ref.shape
    rim_copy = pltpu.make_async_remote_copy(
        pool_ref.at[pl.ds(rows - 16, 16)],
        rim_ref,
        rim_send,
        rim_recv,
        device_id=at(after),
        device_id_type=MESH,
    )

    def weight_copy(k):
        return pltpu.make_async_remote_copy(
            out_weight_ref,
            all_weight_ref.at[tp],
            w_send.at[k],
            w_recv.at[k],
            device_id={"tp": z_peer(k) * 2 + core},
            device_id_type=MESH,
        )

    def weight_forward(k):
        if k == n_z - 1:
            source, target = out_weight_ref, all_weight_ref.at[tp]
        else:
            target = all_weight_ref.at[z_peer(k) * 2 + core]
            source = target
        return pltpu.make_async_remote_copy(
            source,
            target,
            wf_send.at[k],
            wf_recv.at[k],
            device_id={"tp": partner},
            device_id_type=MESH,
        )

    for k in range(n_ep - 1):
        gather_copy(k).start()
    rim_copy.start()
    for k in range(n_z - 1):
        weight_copy(k).start()
    weight_forward(n_z - 1).start()

    def pool():
        padded_ref[: POOL_ROWS - 16] = jnp.zeros((POOL_ROWS - 16, channels), jnp.bfloat16)
        rim_copy.wait_recv()

        @pl.when(place == 0)
        def _():
            padded_ref[POOL_ROWS - 16 : POOL_ROWS] = jnp.zeros((16, channels), jnp.bfloat16)

        @pl.when(place != 0)
        def _():
            padded_ref[POOL_ROWS - 16 : POOL_ROWS] = rim_ref[...]

        padded_ref[POOL_ROWS:] = pool_ref[...]
        group = channels // 4
        reach = (
            lax.broadcasted_iota(jnp.int32, (POOL_ROWS, 2 * POOL_ROWS), 0)
            + POOL_ROWS
            - lax.broadcasted_iota(jnp.int32, (POOL_ROWS, 2 * POOL_ROWS), 1)
        )
        local = lax.broadcasted_iota(jnp.int32, (POOL_ROWS, 1), 0)

        @pl.loop(0, rows // POOL_ROWS)
        def _(i):
            start = pl.multiple_of(i * POOL_ROWS, POOL_ROWS)
            here = pl.ds(start, POOL_ROWS)
            position = place * rows + start + local
            for which, window in enumerate(WINDOWS):
                columns = slice(which * group, (which + 1) * group)
                band = jnp.where((reach >= 0) & (reach < window), 1.0, 0.0).astype(jnp.bfloat16)
                running = jnp.dot(
                    band,
                    padded_ref[pl.ds(start, 2 * POOL_ROWS), columns],
                    preferred_element_type=jnp.float32,
                )
                count = jnp.minimum(position + 1, window).astype(jnp.float32)
                diff = running / count - pool_ref[here, columns].astype(jnp.float32)
                mixed = jnp.dot(
                    diff.astype(jnp.bfloat16),
                    pool_weight_ref[which],
                    preferred_element_type=jnp.float32,
                )
                mixed_ref[here, columns] = (mixed * pool_gain_ref[:, columns]).astype(jnp.bfloat16)

    def project():
        all_weight_ref[tp] = out_weight_ref[...]
        for k in range(n_z - 1):
            weight_copy(k).wait_recv()
            weight_forward(k).start()
        for k in range(n_z):
            weight_forward(k).wait_recv()

        @pl.loop(0, rows // PROJECT_ROWS)
        def _(i):
            here = pl.ds(pl.multiple_of(i * PROJECT_ROWS, PROJECT_ROWS), PROJECT_ROWS)
            projected = jnp.dot(
                mixed_ref[here],
                all_weight_ref[...].reshape(channels, width),
                preferred_element_type=jnp.float32,
            )
            mix_ref[here] = rms_scale(projected, mix_gain_ref[...]).astype(jnp.bfloat16)

    def compute(k, rows):
        lane = lax.broadcasted_iota(jnp.int32, (tokens, LANES), 1) % (LANES // 2)
        packed = rows[:, width:].astype(jnp.float32)

        @pl.loop(0, experts)
        def _(which):
            weight = jnp.sum(
                jnp.where(lane == ep * experts + which, packed, 0.0), axis=1, keepdims=True
            )
            values = rows[:, :width]
            gate = jnp.dot(values, gate_ref[which], preferred_element_type=jnp.float32)
            up = jnp.dot(values, up_ref[which], preferred_element_type=jnp.float32)
            hid_ref[which] = (clamped_unit(gate, up) * weight).astype(jnp.bfloat16)

        @pl.loop(0, tiles)
        def _(j):
            columns = pl.ds(pl.multiple_of(j * TILE, TILE), TILE)
            total = jnp.dot(
                hid_ref[0], down_ref[0, :, columns], preferred_element_type=jnp.float32
            )
            for which in range(1, experts):
                total = total + jnp.dot(
                    hid_ref[which], down_ref[which, :, columns], preferred_element_type=jnp.float32
                )
            part_ref[j] = total.astype(jnp.bfloat16).reshape(part_ref.shape[1:])
            core_copy(k, j).start()

    for load in loads:
        load.wait()
    compute(last, own_ref)

    @pl.loop(0, tiles)
    def _(j):
        core_copy(last, j).wait()
        acc_ref[j] = part_ref[j, :, core].astype(jnp.float32) + core_ref[last, j].astype(
            jnp.float32
        )

    pool()

    @pl.loop(0, n_ep - 1)
    def _(k):
        gather_copy(k).wait_recv()
        forward_copy(k).start()
        forward_copy(k).wait_recv()
        compute(k, x_ref.at[k])

        @pl.loop(0, tiles)
        def _(j):
            core_copy(k, j).wait()
            core_ref[k, j] = (
                part_ref[j, :, core].astype(jnp.float32) + core_ref[k, j].astype(jnp.float32)
            ).astype(jnp.bfloat16)

        peer_copy(k).start()

    project()

    @pl.loop(0, n_ep - 1)
    def _(k):
        peer_copy(k).wait_recv()
        acc_ref[...] += peer_ref[k].astype(jnp.float32)

    for spot in range(n_z):
        zsend_ref[spot] = acc_ref[:, spot].astype(jnp.bfloat16)
    for k in range(n_z - 1):
        z_copy(k).start()
    total = acc_ref[:, z]
    for k in range(n_z - 1):
        z_copy(k).wait_recv()
        total = total + zrecv_ref[k].astype(jnp.float32)
    squares = jnp.sum(jnp.sum(total * total, axis=0), axis=-1, keepdims=True)
    scale = lax.rsqrt(squares / width + EPS)
    for j in range(tiles):
        columns = slice(j * TILE, (j + 1) * TILE)
        out_ref[:, columns] = (total[j] * scale * gain_ref[:, columns]).astype(jnp.bfloat16)

    @pl.loop(0, n_ep - 1)
    def _(k):
        gather_copy(k).wait_send()
        forward_copy(k).wait_send()
        peer_copy(k).wait_send()

    for k in range(n_z - 1):
        z_copy(k).wait_send()
        weight_copy(k).wait_send()
    for k in range(n_z):
        weight_forward(k).wait_send()
    rim_copy.wait_send()


def fused(operands, n_ep, n_tp):
    expert_in, packed, _, gate_weight, up_weight, down_weight = operands[:6]
    pool_in, out_weight = operands[7], operands[10]
    tokens, wide = expert_in.shape[0], expert_in.shape[1] + packed.shape[1]
    rows, channels = pool_in.shape
    experts, width, units = gate_weight.shape
    tiles, n_z, block = width // TILE, n_tp // 2, tokens // n_tp
    dma = pltpu.SemaphoreType.DMA
    vmem = pl.BlockSpec(memory_space=pltpu.VMEM)
    hbm = pl.BlockSpec(memory_space=pl.ANY)
    bf16 = jnp.bfloat16
    return pl.pallas_call(
        functools.partial(expert_kernel, n_ep, n_tp),
        out_shape=(
            jax.ShapeDtypeStruct((rows, width), bf16),
            jax.ShapeDtypeStruct((block, width), bf16),
        ),
        in_specs=[vmem] * 3 + [hbm] * 3 + [vmem] * 6,
        out_specs=(vmem, vmem),
        scratch_shapes=[
            pltpu.VMEM((tokens, wide), bf16),
            pltpu.VMEM((16, channels), bf16),
            pltpu.VMEM((POOL_ROWS + rows, channels), bf16),
            pltpu.VMEM((rows, channels), bf16),
            pltpu.VMEM((n_tp,) + out_weight.shape, bf16),
            pltpu.VMEM((n_ep - 1, tokens, wide), bf16),
            pltpu.VMEM(gate_weight.shape, bf16),
            pltpu.VMEM(up_weight.shape, bf16),
            pltpu.VMEM(down_weight.shape, bf16),
            pltpu.VMEM((experts, tokens, units), bf16),
            pltpu.VMEM((tiles, n_z, 2, block, TILE), bf16),
            pltpu.VMEM((n_ep, tiles, n_z, block, TILE), bf16),
            pltpu.VMEM((n_ep - 1, tiles, n_z, block, TILE), bf16),
            pltpu.VMEM((tiles, n_z, block, TILE), jnp.float32),
            pltpu.VMEM((n_z, tiles, block, TILE), bf16),
            pltpu.VMEM((n_z - 1, tiles, block, TILE), bf16),
            dma((3,)),
            dma((n_ep - 1,)),
            dma((n_ep - 1,)),
            dma((n_ep - 1,)),
            dma((n_ep - 1,)),
            dma((tiles,)),
            dma((n_ep, tiles)),
            dma((n_ep - 1,)),
            dma((n_ep - 1,)),
            dma((n_z - 1,)),
            dma((n_z - 1,)),
            dma,
            dma,
            dma((n_z - 1,)),
            dma((n_z - 1,)),
            dma((n_z,)),
            dma((n_z,)),
        ],
        compiler_params=pltpu.CompilerParams(
            collective_id=0, has_side_effects=True, vmem_limit_bytes=67043328
        ),
        cost_estimate=pl.CostEstimate(
            flops=6 * n_ep * tokens * experts * units * width,
            bytes_accessed=64 * 2**20,
            transcendentals=0,
        ),
        name="experts",
    )(*operands)


def body(
    pool_in,
    pool_weight,
    pool_gain,
    out_weight,
    mix_gain,
    expert_in,
    routes,
    route_weight,
    pre_gain,
    gate_weight,
    up_weight,
    down_weight,
    post_gain,
):
    n_ep, n_tp = lax.axis_size("ep"), lax.axis_size("tp")
    experts = gate_weight.shape[0] * n_ep
    weights = expert_weights(routes, route_weight, experts)
    high = lax.reduce_precision(weights, 8, 7)
    fill = ((0, 0), (0, LANES // 2 - experts))
    packed = jnp.concatenate([jnp.pad(high, fill), jnp.pad(weights - high, fill)], axis=1)
    operands = (
        expert_in,
        packed.astype(jnp.bfloat16),
        pre_gain[None, :],
        gate_weight,
        up_weight,
        down_weight,
        post_gain[None, :],
        pool_in,
        pool_weight,
        pool_gain[None, :],
        out_weight,
        mix_gain[None, :],
    )
    return fused(operands, n_ep, n_tp)


def solution(mesh):
    return jax.shard_map(
        body,
        mesh=mesh,
        in_specs=(
            P(("ep", "tp"), None),
            P(),
            P(),
            P("tp", None),
            P(),
            P("ep", None),
            P("ep", None),
            P("ep", None),
            P(),
            P("ep", None, "tp"),
            P("ep", None, "tp"),
            P("ep", "tp", None),
            P(),
        ),
        out_specs=(P(("ep", "tp"), None), P(("ep", "tp"), None)),
        check_vma=False,
    )
```

profile of v0, /device:TPU:0, one launch (start us, length us, event | category | flops | bytes accessed | tf_op | source)
XLA Modules:
  0.0 80.6 jit_solution(750679530506710918)
XLA Ops:
  0.6 0.7 select_reduce_fusion
  1.4 0.1 copy.20
  1.5 0.1 copy.19
  1.6 0.7 fusion.2.packed_ref
  2.4 74.3 %experts.1 = (bf16[512,2048]{1,0:T(8,128)(2,1)}, bf16[32,2048]{1,0:T(8,128)(2,1)}) custom-call(bf16[256,2048]{1,0:T(8,128)(2,1)} %expert_in_ref.1, bf16[256,128]{1,0:T(8,128)(2,1)} %fusion.2.packed_ref, f32[1,2048]{1,0:T(1,128)} %bitcast.4, bf16[2,2048,512]{2,1,0:T(8,128)(2,1)} %gate_hbm.1, bf16[2,2048,512]{2,1,0:T(8,128)(2,1)} %up_hbm.1, ...), custom_call_target="tpu_custom_call" | custom-call | flops 12884901888 | bytes 67108864 | tf_op jit(solution)/shard_map/experts/pallas_call | solution.py:398
  76.7 0.0 copy-start
  76.7 3.2 %copy.24 = bf16[512,2048]{1,0:T(8,128)(2,1)} copy(bf16[512,2048]{1,0:T(8,128)(2,1)} %get-tuple-element.6) | data formatting | bytes 4194304
  79.9 0.0 copy-done
  79.9 0.7 copy.25
  (2 shorter events, 0.0 us)
Async XLA Ops:
  76.7 3.2 %copy-start = (bf16[32,2048]{1,0:T(8,128)(2,1)S(1)}, bf16[32,2048]{1,0:T(8,128)(2,1)}, u32[]{:S(2)}) copy-start(bf16[32,2048]{1,0:T(8,128)(2,1)} %get-tuple-element.7) | copy-start | bytes 393220
where the time goes:
time: 80.8 us; the launch traced here: 80.6 us
  Pallas kernels  74.3 us (92%)
  local copies, waits for them, and re-layouts  4.1 us (5%)
  other arithmetic  1.47 us (2%)
    pallas_call x1, Pallas kernels, fused(): pl.pallas_call(functools.partial(expert_kernel, n_ep, n_tp), out_shape=(j...  74.3 us
    unnamed x4, local copies, waits for them, and re-layouts  3.85 us

commit v1 on v0

v1 whole, which is shorter than its diff:
```python
import functools
import math

import jax
import jax.numpy as jnp
from jax import lax
from jax.experimental import pallas as pl
from jax.experimental.pallas import tpu as pltpu
from jax.sharding import PartitionSpec as P

WINDOWS = (2, 4, 8, 16)
EPS = 1e-06
LIMIT = 7.0
ALPHA = 1.702
TILE = 256
WIDE = 512
LAG = 2
POOL_ROWS = 128
PROJECT_ROWS = 256
SUBS = 2
MESH = pl.DeviceIdType.MESH


def rms_scale(values, gain):
    mean_square = jnp.mean(values * values, axis=-1, keepdims=True)
    return values * lax.rsqrt(mean_square + EPS) * gain


def clamped_unit(gate, up):
    gate = jnp.minimum(gate, LIMIT)
    up = jnp.clip(up, -LIMIT, LIMIT)
    return (up + 1.0) * gate * jax.nn.sigmoid(ALPHA * gate)


def flipped(place, mask, count):
    result, bit = 0, 1
    while bit < count:
        result = result + ((place // bit + mask // bit) % 2) * bit
        bit *= 2
    return result


def each(count, step):
    if count == 1:
        step(0)
    else:
        pl.loop(0, count)(step)


def both(first, second):
    return jnp.logical_and(first, second)


def mixer_kernel(
    n_ep,
    n_tp,
    expert_hbm,
    routes_ref,
    route_weight_ref,
    pre_gain_ref,
    gate_hbm,
    up_hbm,
    down_hbm,
    gain_ref,
    pool_hbm,
    pool_weight_hbm,
    pool_gain_ref,
    out_weight_hbm,
    mix_gain_ref,
    mix_ref,
    out_ref,
    in_ref,
    own_ref,
    padded_ref,
    mixed_ref,
    pool_weight_ref,
    all_weight_ref,
    own_table_ref,
    table_ref,
    x_ref,
    gate_ref,
    up_ref,
    down_ref,
    hid_ref,
    part_ref,
    core_ref,
    first_ref,
    second_ref,
    acc_ref,
    zsend_ref,
    zrecv_ref,
    load_sem,
    table_send,
    table_recv,
    ag_send,
    ag_recv,
    pair_send,
    pair_recv,
    cs_send,
    cs_recv,
    first_send,
    first_recv,
    second_send,
    second_recv,
    z_send,
    z_recv,
    rim_send,
    rim_recv,
    w_send,
    w_recv,
    wp_send,
    wp_recv,
):
    ep, tp = lax.axis_index("ep"), lax.axis_index("tp")
    core, z = tp % 2, tp // 2
    partner = z * 2 + 1 - core
    n_z = n_tp // 2
    side = math.isqrt(n_ep)
    others = side - 1
    y, x = ep // side, ep % side
    tokens, width = in_ref.shape
    experts = gate_ref.shape[0]
    tiles = width // TILE
    half_tiles = tiles // 2
    half_z = n_z // 2
    piece = tokens // 2
    share = piece // 2
    own = n_ep - 1
    rows = padded_ref.shape[0] - POOL_ROWS
    channels = padded_ref.shape[1]
    sub_rows = out_weight_hbm.shape[0] // SUBS

    def remote(source, target, send, recv, device):
        return pltpu.make_async_remote_copy(
            source, target, send, recv, device_id=device, device_id_type=MESH
        )

    def x_peer(f):
        return {"ep": y * side + flipped(x, f + 1, side)}

    def y_peer(f):
        return {"ep": flipped(y, f + 1, side) * side + x}

    def ep_peer(k):
        return {"ep": flipped(ep, k + 1, n_ep)}

    def z_peer(k):
        return flipped(z, k + 1, n_z)

    place = ep * n_tp + tp
    devices = n_ep * n_tp
    after, before = (place + 1) % devices, (place + devices - 1) % devices

    def at(device):
        return {"ep": device // n_tp, "tp": device % n_tp}

    in_load = pltpu.make_async_copy(expert_hbm, in_ref, load_sem.at[0])
    weight_load = pltpu.make_async_copy(out_weight_hbm, all_weight_ref.at[tp], load_sem.at[1])
    pool_load = pltpu.make_async_copy(
        pool_hbm, padded_ref.at[pl.ds(POOL_ROWS, rows)], load_sem.at[2]
    )
    map_load = pltpu.make_async_copy(pool_weight_hbm, pool_weight_ref, load_sem.at[3])

    def expert_load(e, k):
        source, target = ((gate_hbm, gate_ref), (up_hbm, up_ref), (down_hbm, down_ref))[k]
        return pltpu.make_async_copy(source.at[e], target.at[e], load_sem.at[4 + 3 * e + k])

    for load in (in_load, weight_load, pool_load):
        load.start()
    for e in range(experts):
        for k in range(2):
            expert_load(e, k).start()
    for e in range(experts):
        expert_load(e, 2).start()
    map_load.start()

    barrier = pltpu.get_barrier_semaphore()
    pl.semaphore_signal(barrier, inc=1, device_id=at(after), device_id_type=MESH)
    pl.semaphore_signal(barrier, inc=1, device_id=at(before), device_id_type=MESH)
    pl.semaphore_signal(barrier, inc=1, device_id={"tp": partner}, device_id_type=MESH)
    for k in range(n_ep - 1):
        pl.semaphore_signal(barrier, inc=1, device_id=ep_peer(k), device_id_type=MESH)
    for k in range(n_z - 1):
        pl.semaphore_signal(
            barrier, inc=1, device_id={"tp": z_peer(k) * 2 + core}, device_id_type=MESH
        )

    padded_ref[: POOL_ROWS - 16] = jnp.zeros((POOL_ROWS - 16, channels), jnp.bfloat16)
    lanes = lax.broadcasted_iota(jnp.int32, own_table_ref.shape, 0)
    table = jnp.zeros(own_table_ref.shape, jnp.float32)
    for k in range(routes_ref.shape[0]):
        table = table + jnp.where(
            lanes == routes_ref[k : k + 1, :], route_weight_ref[k : k + 1, :], 0.0
        )
    own_table_ref[...] = table
    in_load.wait()
    own_ref[...] = rms_scale(in_ref[...].astype(jnp.float32), pre_gain_ref[...]).astype(
        jnp.bfloat16
    )
    pl.semaphore_wait(barrier, n_ep + n_z + 1)

    def slot_a(f):
        return f

    def slot_b(f):
        return others + f

    def slot_d(g, f):
        return 2 * others + g * others + f

    def part_rows(p):
        return pl.ds(pl.multiple_of(p * piece + core * share, share), share)

    def gather_copy(source, slot, p, device, sub=None):
        start, size = p * piece + core * share, share
        if sub is not None:
            size = (share // 4, share - share // 4)[sub]
            start = start + sub * (share // 4)
        here = pl.ds(pl.multiple_of(start, share // 4), size)
        k = 0 if sub is None else sub
        return remote(
            source.at[here],
            x_ref.at[slot, here],
            ag_send.at[slot, p, k],
            ag_recv.at[slot, p, k],
            device,
        )

    def early_x(f):
        return gather_copy(own_ref, slot_a(f), 0, x_peer(f))

    def early_y(f):
        return gather_copy(own_ref, slot_a(f), 1, y_peer(f))

    def late_x(f, sub):
        return gather_copy(own_ref, slot_b(f), 1, x_peer(f), sub)

    def late_y(f, sub):
        return gather_copy(own_ref, slot_b(f), 0, y_peer(f), sub)

    def pass_y(g, f):
        return gather_copy(x_ref.at[slot_a(f)], slot_d(g, f), 0, y_peer(g))

    def pass_x(g, f):
        return gather_copy(x_ref.at[slot_a(g)], slot_d(g, f), 1, x_peer(f))

    def pair_copy(slot, p):
        here = part_rows(p)
        return remote(
            x_ref.at[slot, here],
            x_ref.at[slot, here],
            pair_send.at[slot, p],
            pair_recv.at[slot, p],
            {"tp": partner},
        )

    def table_copy(k):
        return remote(
            own_table_ref, table_ref.at[k], table_send.at[k], table_recv.at[k], ep_peer(k)
        )

    def core_copy(slot, j):
        return remote(
            part_ref.at[j, :, 1 - core],
            core_ref.at[slot, j],
            cs_send.at[j],
            cs_recv.at[slot, j],
            {"tp": partner},
        )

    def z_rows(p):
        return pl.ds(p * half_z, half_z)

    def first_copy(h, f, g, jj, p, slot):
        return remote(
            core_ref.at[slot, h * half_tiles + jj, z_rows(p)],
            first_ref.at[h, f, g, jj, p],
            first_send.at[h, f, g, jj, p],
            first_recv.at[h, f, g, jj, p],
            x_peer(f) if h == 0 else y_peer(f),
        )

    def second_slot(h, g, p):
        return slot_a(g) if h != p else slot_b(g)

    def second_copy(h, g, jj, p):
        return remote(
            core_ref.at[second_slot(h, g, p), h * half_tiles + jj, z_rows(p)],
            second_ref.at[h, g, jj, p],
            second_send.at[h, g, jj, p],
            second_recv.at[h, g, jj, p],
            y_peer(g) if h == 0 else x_peer(g),
        )

    levels = n_z.bit_length() - 1

    def z_part(level):
        count = n_z >> (level + 1)
        return (z // (1 << level)) % 2, n_z - 2 * count, count

    def z_copy(level, j):
        _, first, count = z_part(level)
        return remote(
            zsend_ref.at[j, pl.ds(first, count)],
            zrecv_ref.at[j, pl.ds(first, count)],
            z_send.at[level, j],
            z_recv.at[level, j],
            {"tp": flipped(z, 1 << level, n_z) * 2 + core},
        )

    rim_copy = remote(
        padded_ref.at[pl.ds(POOL_ROWS + rows - 16, 16)],
        padded_ref.at[pl.ds(POOL_ROWS - 16, 16)],
        rim_send,
        rim_recv,
        at(after),
    )

    def weight_rows(block, sub):
        return all_weight_ref.at[block, pl.ds(sub * sub_rows, sub_rows)]

    def toward(d, s):
        return z - s if d == 0 else z + s

    def sends(d, s):
        if d == 0:
            return both(z + 1 < n_z, z - s >= 0)
        return both(z >= 1, z + s < n_z)

    def receives(d, s):
        return z - 1 - s >= 0 if d == 0 else z + 1 + s < n_z

    def weight_copy(d, s, sub):
        block = weight_rows(toward(d, s) * 2 + core, sub)
        target = z + 1 if d == 0 else z - 1
        return remote(
            block, block, w_send.at[d, s, sub], w_recv.at[d, s, sub], {"tp": target * 2 + core}
        )

    def weight_arrival(d, s, sub):
        block = weight_rows(toward(d, s + 1) * 2 + core, sub)
        return remote(
            block, block, w_send.at[d, s, sub], w_recv.at[d, s, sub], {"tp": partner}
        )

    def weight_pair(d, s, sub):
        block = weight_rows(toward(d, s + 1) * 2 + core, sub)
        k = 1 + d * (n_z - 1) + s
        return remote(block, block, wp_send.at[k, sub], wp_recv.at[k, sub], {"tp": partner})

    def own_pair(sub):
        block = weight_rows(tp, sub)
        return remote(block, block, wp_send.at[0, sub], wp_recv.at[0, sub], {"tp": partner})

    def weight_step(s, sub):
        for d in range(2):

            @pl.when(receives(d, s))
            def _():
                weight_arrival(d, s, sub).wait_recv()
                weight_pair(d, s, sub).start()

            if s + 1 < n_z - 1:

                @pl.when(sends(d, s + 1))
                def _():
                    weight_copy(d, s + 1, sub).start()

    for f in range(others):
        early_x(f).start()
        early_y(f).start()
    for k in range(n_ep - 1):
        table_copy(k).start()
    for f in range(others):
        late_x(f, 0).start()
        late_y(f, 0).start()
    pool_load.wait()
    rim_copy.start()
    weight_load.wait()
    for sub in range(SUBS):
        for d in range(2):

            @pl.when(sends(d, 0))
            def _():
                weight_copy(d, 0, sub).start()

        own_pair(sub).start()

    def pool():
        rim_copy.wait_recv()

        @pl.when(place == 0)
        def _():
            padded_ref[POOL_ROWS - 16 : POOL_ROWS] = jnp.zeros((16, channels), jnp.bfloat16)

        map_load.wait()
        group = channels // 4
        reach = (
            lax.broadcasted_iota(jnp.int32, (POOL_ROWS, 2 * POOL_ROWS), 0)
            + POOL_ROWS
            - lax.broadcasted_iota(jnp.int32, (POOL_ROWS, 2 * POOL_ROWS), 1)
        )
        local = lax.broadcasted_iota(jnp.int32, (POOL_ROWS, 1), 0)

        @pl.loop(0, rows // POOL_ROWS)
        def _(i):
            start = pl.multiple_of(i * POOL_ROWS, POOL_ROWS)
            here = pl.ds(start, POOL_ROWS)
            there = pl.ds(start + POOL_ROWS, POOL_ROWS)
            position = place * rows + start + local
            for which, window in enumerate(WINDOWS):
                columns = slice(which * group, (which + 1) * group)
                band = jnp.where((reach >= 0) & (reach < window), 1.0, 0.0).astype(jnp.bfloat16)
                running = jnp.dot(
                    band,
                    padded_ref[pl.ds(start, 2 * POOL_ROWS), columns],
                    preferred_element_type=jnp.float32,
                )
                count = jnp.minimum(position + 1, window).astype(jnp.float32)
                diff = running / count - padded_ref[there, columns].astype(jnp.float32)
                mixed = jnp.dot(
                    diff.astype(jnp.bfloat16),
                    pool_weight_ref[which],
                    preferred_element_type=jnp.float32,
                )
                mixed_ref[here, columns] = (mixed * pool_gain_ref[:, columns]).astype(jnp.bfloat16)

    def project(i):
        here = pl.ds(pl.multiple_of(i * PROJECT_ROWS, PROJECT_ROWS), PROJECT_ROWS)
        projected = jnp.dot(
            mixed_ref[here],
            all_weight_ref[...].reshape(channels, width),
            preferred_element_type=jnp.float32,
        )
        mix_ref[here] = rms_scale(projected, mix_gain_ref[...]).astype(jnp.bfloat16)

    def hidden(values_ref, table, first=False):
        lane = lax.broadcasted_iota(jnp.int32, (tokens, table.shape[0]), 1)
        weights = jnp.transpose(table)
        for which in range(experts):
            if first:
                for k in range(2):
                    expert_load(which, k).wait()
            weight = jnp.sum(
                jnp.where(lane == ep * experts + which, weights, 0.0), axis=1, keepdims=True
            )
            values = values_ref[...]
            gate = jnp.dot(values, gate_ref[which], preferred_element_type=jnp.float32)
            up = jnp.dot(values, up_ref[which], preferred_element_type=jnp.float32)
            hid_ref[which] = (clamped_unit(gate, up) * weight).astype(jnp.bfloat16)

    def partial(slot, after, lag=LAG, hook=None):
        def ended(j):
            for k in range(WIDE // TILE):
                core_copy(slot, j + k).wait()
                after((j + k) // half_tiles, (j + k) % half_tiles)

        starts = [
            h * half_tiles + jj for jj in range(0, half_tiles, WIDE // TILE) for h in range(2)
        ]
        for i, j in enumerate(starts):
            columns = slice(j * TILE, j * TILE + WIDE)
            total = jnp.dot(
                hid_ref[0], down_ref[0, :, columns], preferred_element_type=jnp.float32
            )
            for which in range(1, experts):
                total = total + jnp.dot(
                    hid_ref[which], down_ref[which, :, columns], preferred_element_type=jnp.float32
                )
            total = total.astype(jnp.bfloat16)
            for k in range(WIDE // TILE):
                part_ref[j + k] = total[:, k * TILE : (k + 1) * TILE].reshape(part_ref.shape[1:])
                core_copy(slot, j + k).start()
            if i >= lag:
                ended(starts[i - lag])
        if hook is not None:
            hook()
        for j in starts[len(starts) - lag :]:
            ended(j)

    def joined(k0, k1):
        return jnp.concatenate(
            [table_ref[k0, :, :piece], table_ref[k1, :, piece:]], axis=1
        )

    def core_sum(slot, h, jj):
        j = h * half_tiles + jj
        return part_ref[j, :, core].astype(jnp.float32) + core_ref[slot, j].astype(jnp.float32)

    hidden(own_ref, own_table_ref[...], first=True)
    pool()
    for e in range(experts):
        expert_load(e, 2).wait()

    def own_done(h, jj):
        acc_ref[h * half_tiles + jj] = core_sum(own, h, jj)

    steps = [(s, sub) for s in range(n_z - 1) for sub in range(SUBS)]
    last = width // WIDE

    def early_arrived():
        for f in range(others):
            early_x(f).wait_recv()
            early_y(f).wait_recv()
            for g in range(others):
                pass_y(g, f).start()
                pass_x(f, g).start()
            for p in range(2):
                pair_copy(slot_a(f), p).start()
        for f in range(others):
            late_x(f, 1).start()
            late_y(f, 1).start()
        weight_step(*steps[0])

    partial(own, own_done, last, early_arrived)
    for k in range(n_ep - 1):
        table_copy(k).wait_recv()

    def halves():
        return [(h, jj) for jj in range(half_tiles) for h in range(2)]

    def late_pairs():
        for f in range(others):
            for sub in range(2):
                late_x(f, sub).wait_recv()
                late_y(f, sub).wait_recv()
            for p in range(2):
                pair_copy(slot_b(f), p).start()

    def diagonal_pairs():
        for g in range(others):
            for f in range(others):
                pass_y(g, f).wait_recv()
                pass_x(g, f).wait_recv()
                for p in range(2):
                    pair_copy(slot_d(g, f), p).start()

    def batch(slot, k0, k1, send, lag=LAG, hook=None):
        for p in range(2):
            pair_copy(slot, p).wait_recv()
        hidden(x_ref.at[slot], joined(k0, k1))

        def done(h, jj):
            core_ref[slot, h * half_tiles + jj] = core_sum(slot, h, jj).astype(jnp.bfloat16)
            send(h, jj)

        partial(slot, done, lag, hook if others == 1 else None)

    def batch_a(f):
        def send(h, jj):
            first_copy(h, f, 0, jj, h, slot_a(f)).start()

        batch(slot_a(f), f, (f + 1) * side - 1, send, last, diagonal_pairs)

    def batch_d(i):
        g, f = (i // others, i % others) if others > 1 else (0, 0)

        def send(h, jj):
            for p in range(2):
                if h == 0:
                    first_copy(0, f, g + 1, jj, p, slot_d(g, f)).start()
                else:
                    first_copy(1, g, f + 1, jj, p, slot_d(g, f)).start()

        k = (g + 1) * side + f
        batch(slot_d(g, f), k, k, send, LAG, late_pairs)

    def batch_b(f):
        def send(h, jj):
            first_copy(h, f, 0, jj, 1 - h, slot_b(f)).start()

        batch(slot_b(f), (f + 1) * side - 1, f, send)

    each(others, batch_a)
    if others > 1:
        diagonal_pairs()
    weight_step(*steps[1])
    each(others * others, batch_d)
    if others > 1:
        late_pairs()
    weight_step(*steps[2])
    each(others, batch_b)
    weight_step(*steps[3])

    def second_stage(g):
        for late, (h, jj) in [(late, tile) for late in range(2) for tile in halves()]:
            for p in (h if late else 1 - h,):
                slot, j = second_slot(h, g, p), h * half_tiles + jj
                total = core_ref[slot, j, z_rows(p)].astype(jnp.float32)
                for f in range(others):
                    first_copy(h, f, g + 1, jj, p, slot).wait_recv()
                    total = total + first_ref[h, f, g + 1, jj, p].astype(jnp.float32)
                core_ref[slot, j, z_rows(p)] = total.astype(jnp.bfloat16)
                second_copy(h, g, jj, p).start()

    each(others, second_stage)

    def plane_sum(j, h, jj):
        for p in range(2):
            total = acc_ref[j, z_rows(p)]
            for f in range(others):
                first_copy(h, f, 0, jj, p, own).wait_recv()
                total = total + first_ref[h, f, 0, jj, p].astype(jnp.float32)
            for g in range(others):
                second_copy(h, g, jj, p).wait_recv()
                total = total + second_ref[h, g, jj, p].astype(jnp.float32)
            acc_ref[j, z_rows(p)] = total

    def z_level(level, jj):
        for h in range(2):
            j = h * half_tiles + jj
            if level == 0:
                plane_sum(j, h, jj)
            else:
                z_fold(level - 1, j)
            if level < levels:
                bit, first, count = z_part(level)
                for m in range(count):
                    zsend_ref[j, first + m] = acc_ref[j, 2 * m + 1 - bit].astype(jnp.bfloat16)
                z_copy(level, j).start()

    def z_fold(level, j):
        bit, first, count = z_part(level)
        z_copy(level, j).wait_recv()
        for m in range(count):
            acc_ref[j, m] = acc_ref[j, 2 * m + bit] + zrecv_ref[j, first + m].astype(jnp.float32)

    waves = [(level, jj) for level in range(levels) for jj in range(half_tiles)]
    waves.sort(key=lambda wave: (wave[1] + 3 * wave[0], wave[0]))
    rest = steps[4:]
    for wave in waves:
        z_level(*wave)
        if rest:
            weight_step(*rest.pop(0))
    for step in rest:
        weight_step(*step)
    for sub in range(SUBS):
        own_pair(sub).wait_recv()
        for s in range(n_z - 1):
            for d in range(2):

                @pl.when(receives(d, s))
                def _():
                    weight_pair(d, s, sub).wait_recv()

    pl.loop(0, rows // PROJECT_ROWS)(project)

    squares = 0.0
    for jj in range(half_tiles):
        z_level(levels, jj)
        for h in range(2):
            total = acc_ref[h * half_tiles + jj, 0]
            squares = squares + jnp.sum(total * total, axis=-1, keepdims=True)
    scale = lax.rsqrt(squares / width + EPS)
    for j in range(tiles):
        columns = slice(j * TILE, (j + 1) * TILE)
        out_ref[:, columns] = (acc_ref[j, 0] * scale * gain_ref[:, columns]).astype(jnp.bfloat16)

    for f in range(others):
        early_x(f).wait_send()
        early_y(f).wait_send()
        for sub in range(2):
            late_x(f, sub).wait_send()
            late_y(f, sub).wait_send()
        for g in range(others):
            pass_y(g, f).wait_send()
            pass_x(g, f).wait_send()

    @pl.loop(0, n_ep - 1)
    def _(k):
        table_copy(k).wait_send()
        for p in range(2):
            pair_copy(k, p).wait_send()

    for h in range(2):
        for f in range(others):
            for jj in range(half_tiles):
                for p in range(2):
                    for g in range(side):
                        first_copy(h, f, g, jj, p, own).wait_send()
                    second_copy(h, f, jj, p).wait_send()
    for j in range(tiles):
        for level in range(levels):
            z_copy(level, j).wait_send()
    for sub in range(SUBS):
        own_pair(sub).wait_send()
        for s in range(n_z - 1):
            for d in range(2):

                @pl.when(sends(d, s))
                def _():
                    weight_copy(d, s, sub).wait_send()

                @pl.when(receives(d, s))
                def _():
                    weight_pair(d, s, sub).wait_send()

    rim_copy.wait_send()


def fused(operands, n_ep, n_tp):
    expert_in, routes, _, _, gate_weight, up_weight, down_weight = operands[:7]
    pool_in, pool_weight, out_weight = operands[8], operands[9], operands[11]
    tokens, width = expert_in.shape
    rows, channels = pool_in.shape
    experts, _, units = gate_weight.shape
    tiles, n_z, block = width // TILE, n_tp // 2, tokens // n_tp
    side = math.isqrt(n_ep)
    others, half_tiles, half_z = side - 1, tiles // 2, n_z // 2
    dma = pltpu.SemaphoreType.DMA
    vmem = pl.BlockSpec(memory_space=pltpu.VMEM)
    hbm = pl.BlockSpec(memory_space=pltpu.HBM)
    bf16, f32 = jnp.bfloat16, jnp.float32
    buffers = [
        ((tokens, width), bf16),
        ((tokens, width), bf16),
        ((POOL_ROWS + rows, channels), bf16),
        ((rows, channels), bf16),
        (pool_weight.shape, bf16),
        ((n_tp,) + out_weight.shape, bf16),
        ((n_ep * experts, tokens), f32),
        ((n_ep - 1, n_ep * experts, tokens), f32),
        ((n_ep - 1, tokens, width), bf16),
        (gate_weight.shape, bf16),
        (up_weight.shape, bf16),
        (down_weight.shape, bf16),
        ((experts, tokens, units), bf16),
        ((tiles, n_z, 2, block, TILE), bf16),
        ((n_ep, tiles, n_z, block, TILE), bf16),
        ((2, others, side, half_tiles, 2, half_z, block, TILE), bf16),
        ((2, others, half_tiles, 2, half_z, block, TILE), bf16),
        ((tiles, n_z, block, TILE), f32),
        ((tiles, n_z - 1, block, TILE), bf16),
        ((tiles, n_z - 1, block, TILE), bf16),
    ]
    held = sum(math.prod(shape) * jnp.dtype(kind).itemsize for shape, kind in buffers)
    return pl.pallas_call(
        functools.partial(mixer_kernel, n_ep, n_tp),
        out_shape=(pltpu.VMEM((rows, width), bf16), pltpu.VMEM((block, width), bf16)),
        in_specs=[hbm, vmem, vmem, vmem, hbm, hbm, hbm, vmem, hbm, hbm, vmem, hbm, vmem],
        out_specs=(vmem, vmem),
        scratch_shapes=[pltpu.VMEM(shape, kind) for shape, kind in buffers]
        + [
            dma((4 + 3 * experts,)),
            dma((n_ep - 1,)),
            dma((n_ep - 1,)),
            dma((n_ep - 1, 2, 2)),
            dma((n_ep - 1, 2, 2)),
            dma((n_ep - 1, 2)),
            dma((n_ep - 1, 2)),
            dma((tiles,)),
            dma((n_ep, tiles)),
            dma((2, others, side, half_tiles, 2)),
            dma((2, others, side, half_tiles, 2)),
            dma((2, others, half_tiles, 2)),
            dma((2, others, half_tiles, 2)),
            dma((n_z - 1, tiles)),
            dma((n_z - 1, tiles)),
            dma,
            dma,
            dma((2, n_z - 1, SUBS)),
            dma((2, n_z - 1, SUBS)),
            dma((2 * n_z - 1, SUBS)),
            dma((2 * n_z - 1, SUBS)),
        ],
        compiler_params=pltpu.CompilerParams(
            collective_id=0,
            has_side_effects=True,
            vmem_limit_bytes=min(67043328, held + 10 * 2**20),
        ),
        cost_estimate=pl.CostEstimate(
            flops=6 * n_ep * tokens * experts * units * width,
            bytes_accessed=64 * 2**20,
            transcendentals=0,
        ),
        name="mixer_experts",
    )(*(pltpu.with_memory_space_constraint(operand, pltpu.HBM) for operand in operands))


def body(
    pool_in,
    pool_weight,
    pool_gain,
    out_weight,
    mix_gain,
    expert_in,
    routes,
    route_weight,
    pre_gain,
    gate_weight,
    up_weight,
    down_weight,
    post_gain,
):
    n_ep, n_tp = lax.axis_size("ep"), lax.axis_size("tp")
    operands = (
        expert_in,
        routes.T,
        route_weight.T,
        pre_gain[None, :],
        gate_weight,
        up_weight,
        down_weight,
        post_gain[None, :],
        pool_in,
        pool_weight,
        pool_gain[None, :],
        out_weight,
        mix_gain[None, :],
    )
    return fused(operands, n_ep, n_tp)


def solution(mesh):
    return jax.shard_map(
        body,
        mesh=mesh,
        in_specs=(
            P(("ep", "tp"), None),
            P(),
            P(),
            P("tp", None),
            P(),
            P("ep", None),
            P("ep", None),
            P("ep", None),
            P(),
            P("ep", None, "tp"),
            P("ep", None, "tp"),
            P("ep", "tp", None),
            P(),
        ),
        out_specs=(P(("ep", "tp"), None), P(("ep", "tp"), None)),
        check_vma=False,
    )
```

time: 80.8 us -> 60.8 us (0.75)
  Pallas kernels: 74.3 us -> 58 us
  local copies, waits for them, and re-layouts: 4.1 us -> 1.98 us
  other arithmetic: 1.47 us -> 0 us
    pallas_call x1, Pallas kernels: 74.3 us -> 58 us  [fused(): pl.pallas_call(functools.partial(mixer_kernel, n_ep, n_tp), out_shape=(pl...]
    unnamed x4 -> x2, local copies, waits for them, and re-layouts: 3.85 us -> 1.98 us
where the time goes in v1:
time: 60.8 us; the launch traced here: 60.6 us
  Pallas kernels  58 us (95%)
  local copies, waits for them, and re-layouts  1.98 us (3%)
  between operations  0.64 us (1%)
    pallas_call x1, Pallas kernels, fused(): pl.pallas_call(functools.partial(mixer_kernel, n_ep, n_tp), out_shape=(pl...  58 us
    unnamed x2, local copies, waits for them, and re-layouts  1.98 us

profile of v1, /device:TPU:0, one launch (start us, length us, event | category | flops | bytes accessed | tf_op | source)
XLA Modules:
  0.0 60.6 jit_solution(4788472552632050261)
XLA Ops:
  0.6 58.0 %mixer_experts.1 = (bf16[512,2048]{1,0:T(8,128)(2,1)S(1)}, bf16[32,2048]{1,0:T(8,128)(2,1)S(1)}) custom-call(bf16[256,2048]{1,0:T(8,128)(2,1)} %expert_hbm.1, s32[4,256]{1,0:T(4,128)} %bitcast.9, f32[4,256]{1,0:T(4,128)} %bitcast.10, f32[1,2048]{1,0:T(1,128)} %bitcast.6, bf16[2,2048,512]{2,1,0:T(8,128)(2,1)} %gate_hbm.1, bf16[2,2048,512]{2,1,0:T(8,128)(2,1)} %up_hbm.1, ...), custom_call_target="tpu_custom_call" | custom-call | flops 12884901888 | bytes 67108864 | tf_op jit(solution)/shard_map/mixer_experts/pallas_call | solution.py:737
  58.6 1.3 %copy.17 = bf16[512,2048]{1,0:T(8,128)(2,1)} copy(bf16[512,2048]{1,0:T(8,128)(2,1)S(1)} %get-tuple-element.2) | data formatting | bytes 4194304
  59.9 0.7 %copy.18 = bf16[32,2048]{1,0:T(8,128)(2,1)} copy(bf16[32,2048]{1,0:T(8,128)(2,1)S(1)} %get-tuple-element.3) | data formatting | bytes 262144

commit v2 on v1

v2 whole, which is shorter than its diff:
```python
import functools
import math

import jax
import jax.numpy as jnp
from jax import lax
from jax.experimental import pallas as pl
from jax.experimental.pallas import tpu as pltpu
from jax.sharding import PartitionSpec as P

WINDOWS = (2, 4, 8, 16)
EPS = 1e-06
LIMIT = 7.0
ALPHA = 1.702
TILE = 256
WIDE = 512
LAG = 2
POOL_ROWS = 128
PROJECT_ROWS = 256
SUBS = 4
MESH = pl.DeviceIdType.MESH


def rms_scale(values, gain):
    mean_square = jnp.mean(values * values, axis=-1, keepdims=True)
    return values * lax.rsqrt(mean_square + EPS) * gain


def clamped_unit(gate, up):
    gate = jnp.minimum(gate, LIMIT)
    up = jnp.clip(up, -LIMIT, LIMIT)
    return (up + 1.0) * gate * jax.nn.sigmoid(ALPHA * gate)


def flipped(place, mask, count):
    result, bit = 0, 1
    while bit < count:
        result = result + ((place // bit + mask // bit) % 2) * bit
        bit *= 2
    return result


def each(count, step):
    if count == 1:
        step(0)
    else:
        pl.loop(0, count)(step)


def both(first, second):
    return jnp.logical_and(first, second)


def mixer_kernel(
    n_ep,
    n_tp,
    expert_hbm,
    routes_hbm,
    route_weight_hbm,
    pre_gain_hbm,
    gate_hbm,
    up_hbm,
    down_hbm,
    gain_hbm,
    pool_hbm,
    pool_weight_hbm,
    pool_gain_hbm,
    out_weight_hbm,
    mix_gain_hbm,
    mix_ref,
    out_ref,
    routes_ref,
    route_weight_ref,
    pre_gain_ref,
    gain_ref,
    pool_gain_ref,
    mix_gain_ref,
    in_ref,
    own_ref,
    padded_ref,
    mixed_ref,
    pool_weight_ref,
    all_weight_ref,
    own_table_ref,
    table_ref,
    x_ref,
    gate_ref,
    up_ref,
    down_ref,
    hid_ref,
    part_ref,
    core_ref,
    first_ref,
    second_ref,
    acc_ref,
    zsend_ref,
    zrecv_ref,
    ysend_ref,
    yrecv_ref,
    load_sem,
    table_send,
    table_recv,
    ag_send,
    ag_recv,
    pair_send,
    pair_recv,
    cs_send,
    cs_recv,
    first_send,
    first_recv,
    second_send,
    second_recv,
    z_send,
    z_recv,
    y_send,
    y_recv,
    rim_send,
    rim_recv,
    w_send,
    w_recv,
    wp_send,
    wp_recv,
):
    ep, tp = lax.axis_index("ep"), lax.axis_index("tp")
    core, z = tp % 2, tp // 2
    partner = z * 2 + 1 - core
    n_z = n_tp // 2
    side = math.isqrt(n_ep)
    others = side - 1
    y, x = ep // side, ep % side
    tokens, width = in_ref.shape
    experts = gate_ref.shape[0]
    tiles = width // TILE
    half_tiles = tiles // 2
    half_z = n_z // 2
    piece = tokens // 2
    share = piece // 2
    own = n_ep - 1
    pack = WIDE // TILE
    rows = padded_ref.shape[0] - POOL_ROWS
    channels = padded_ref.shape[1]
    sub_rows = out_weight_hbm.shape[0] // SUBS

    def remote(source, target, send, recv, device):
        return pltpu.make_async_remote_copy(
            source, target, send, recv, device_id=device, device_id_type=MESH
        )

    def x_peer(f):
        return {"ep": y * side + flipped(x, f + 1, side)}

    def y_peer(f):
        return {"ep": flipped(y, f + 1, side) * side + x}

    def ep_peer(k):
        return {"ep": flipped(ep, k + 1, n_ep)}

    def z_peer(k):
        return flipped(z, k + 1, n_z)

    place = ep * n_tp + tp
    devices = n_ep * n_tp
    after, before = (place + 1) % devices, (place + devices - 1) % devices

    def at(device):
        return {"ep": device // n_tp, "tp": device % n_tp}

    barrier = pltpu.get_barrier_semaphore()
    pl.semaphore_signal(barrier, inc=1, device_id=at(after), device_id_type=MESH)
    pl.semaphore_signal(barrier, inc=1, device_id=at(before), device_id_type=MESH)
    pl.semaphore_signal(barrier, inc=1, device_id={"tp": partner}, device_id_type=MESH)
    for k in range(n_ep - 1):
        pl.semaphore_signal(barrier, inc=1, device_id=ep_peer(k), device_id_type=MESH)
    for k in range(n_z - 1):
        pl.semaphore_signal(
            barrier, inc=1, device_id={"tp": z_peer(k) * 2 + core}, device_id_type=MESH
        )

    quarters = [
        pl.ds(pl.multiple_of(p * piece + side_of * share, share), share)
        for side_of in (core, 1 - core)
        for p in range(2)
    ]
    pairs = (
        (pre_gain_hbm, pre_gain_ref),
        *((expert_hbm.at[rows_of], in_ref.at[rows_of]) for rows_of in quarters),
        (routes_hbm, routes_ref),
        (route_weight_hbm, route_weight_ref),
        (out_weight_hbm, all_weight_ref.at[tp]),
        (pool_hbm, padded_ref.at[pl.ds(POOL_ROWS, rows)]),
        (pool_weight_hbm, pool_weight_ref),
        (pool_gain_hbm, pool_gain_ref),
        (gain_hbm, gain_ref),
        (mix_gain_hbm, mix_gain_ref),
    )
    loads = [
        pltpu.make_async_copy(source, target, load_sem.at[k])
        for k, (source, target) in enumerate(pairs)
    ]

    def expert_load(e, k):
        source, target = ((gate_hbm, gate_ref), (up_hbm, up_ref), (down_hbm, down_ref))[k]
        return pltpu.make_async_copy(
            source.at[e], target.at[e], load_sem.at[len(pairs) + 3 * e + k]
        )

    for k in (0, 1, 2, 8, 3, 4, 5, 6, 7):
        loads[k].start()
    for e in range(experts):
        for k in range(2):
            expert_load(e, k).start()
    for load in loads[9:]:
        load.start()
    for e in range(experts):
        expert_load(e, 2).start()

    def norm(rows_of):
        own_ref[rows_of] = rms_scale(
            in_ref[rows_of].astype(jnp.float32), pre_gain_ref[...]
        ).astype(jnp.bfloat16)

    loads[0].wait()
    for k in range(2):
        loads[1 + k].wait()
        norm(quarters[k])
    pl.semaphore_wait(barrier, n_ep + n_z + 1)

    def slot_a(f):
        return f

    def slot_d(g, f):
        return others + g * others + f

    def slot_b(f):
        return others + others * others + f

    def turn(slot):
        return (slot + 1) % n_ep % 2

    def part_rows(p):
        return pl.ds(pl.multiple_of(p * piece + core * share, share), share)

    def half_rows(p, sub):
        size = share // 2
        return pl.ds(pl.multiple_of(p * piece + core * share + sub * size, size), size)

    def gather_copy(source, slot, p, sub, device, together=False):
        here = half_rows(p, sub)
        return remote(
            source.at[here],
            x_ref.at[slot, here],
            ag_send,
            ag_recv.at[slot, 0 if together else sub],
            device,
        )

    def gathered(slot, sub, count):
        here = x_ref.at[slot, pl.ds(0, count)]
        return remote(here, here, ag_send, ag_recv.at[slot, sub], {"tp": partner})

    def early_x(f, sub):
        return gather_copy(own_ref, slot_a(f), 0, sub, x_peer(f))

    def early_y(f, sub):
        return gather_copy(own_ref, slot_a(f), 1, sub, y_peer(f))

    def late_x(f, sub):
        return gather_copy(own_ref, slot_b(f), 1, sub, x_peer(f), True)

    def late_y(f, sub):
        return gather_copy(own_ref, slot_b(f), 0, sub, y_peer(f), True)

    def pass_y(g, f, sub):
        return gather_copy(x_ref.at[slot_a(f)], slot_d(g, f), 0, sub, y_peer(g))

    def pass_x(g, f, sub):
        return gather_copy(x_ref.at[slot_a(g)], slot_d(g, f), 1, sub, x_peer(f))

    def pair_copy(slot, p, sub):
        here = half_rows(p, sub)
        return remote(
            x_ref.at[slot, here],
            x_ref.at[slot, here],
            pair_send,
            pair_recv.at[slot],
            {"tp": partner},
        )

    def paired(slot):
        here = x_ref.at[slot, pl.ds(0, piece)]
        return remote(here, here, pair_send, pair_recv.at[slot], {"tp": partner})

    def table_copy(k):
        return remote(
            own_table_ref, table_ref.at[k], table_send, table_recv, ep_peer(k)
        )

    def core_copy(slot, j):
        return remote(
            part_ref.at[pl.ds(j, pack), :, 1 - core],
            core_ref.at[slot, pl.ds(j, pack)],
            cs_send,
            cs_recv.at[turn(slot), j // pack],
            {"tp": partner},
        )

    def core_sent(slot):
        return remote(core_ref.at[slot], core_ref.at[slot], cs_send, rim_recv, {"tp": partner})

    def z_rows(p):
        return pl.ds(p * half_z, half_z)

    def first_copy(h, f, g, jj, p, slot):
        return remote(
            core_ref.at[slot, h * half_tiles + jj, z_rows(p)],
            first_ref.at[h, f, g, jj, z_rows(p)],
            first_send,
            first_recv.at[h, f, g, jj],
            x_peer(f) if h == 0 else y_peer(f),
        )

    def whole_copy(h, f, g, jj, slot):
        return remote(
            core_ref.at[slot, h * half_tiles + jj],
            first_ref.at[h, f, g, jj],
            first_send,
            first_recv.at[h, f, g, jj],
            x_peer(f) if h == 0 else y_peer(f),
        )

    def second_slot(h, g, p):
        return slot_a(g) if h != p else slot_b(g)

    def second_copy(h, g, jj, p):
        return remote(
            core_ref.at[second_slot(h, g, p), h * half_tiles + jj, z_rows(p)],
            second_ref.at[h, g, jj, z_rows(p)],
            second_send,
            second_recv.at[h, g, jj],
            y_peer(g) if h == 0 else x_peer(g),
        )

    def second_arrival(h, g, jj):
        here = second_ref.at[h, g, jj]
        return remote(here, here, second_send, second_recv.at[h, g, jj], {"tp": partner})

    levels = n_z.bit_length() - 1

    def z_part(level):
        count = n_z >> (level + 1)
        return (z // (1 << level)) % 2, n_z - 2 * count, count

    def z_copy(level, j):
        _, first, count = z_part(level)
        return remote(
            zsend_ref.at[j, pl.ds(first, count)],
            zrecv_ref.at[j, pl.ds(first, count)],
            z_send,
            z_recv.at[level, j],
            {"tp": flipped(z, 1 << level, n_z) * 2 + core},
        )

    rim_copy = remote(
        padded_ref.at[pl.ds(POOL_ROWS + rows - 16, 16)],
        padded_ref.at[pl.ds(POOL_ROWS - 16, 16)],
        rim_send,
        rim_recv,
        at(after),
    )

    def weight_rows(block, sub):
        return all_weight_ref.at[block, pl.ds(sub * sub_rows, sub_rows)]

    def toward(d, s):
        return z - s if d == 0 else z + s

    def sends(d, s):
        if d == 0:
            return both(z + 1 < n_z, z - s >= 0)
        return both(z >= 1, z + s < n_z)

    def receives(d, s):
        return z - 1 - s >= 0 if d == 0 else z + 1 + s < n_z

    def weight_copy(d, s, sub):
        block = weight_rows(toward(d, s) * 2 + core, sub)
        target = z + 1 if d == 0 else z - 1
        return remote(
            block, block, w_send, w_recv.at[d, s, sub], {"tp": target * 2 + core}
        )

    def weight_arrival(d, s, sub):
        block = weight_rows(toward(d, s + 1) * 2 + core, sub)
        return remote(
            block, block, w_send, w_recv.at[d, s, sub], {"tp": partner}
        )

    def weight_pair(d, s, sub):
        block = weight_rows(toward(d, s + 1) * 2 + core, sub)
        return remote(block, block, wp_send, wp_recv, {"tp": partner})

    def own_pair(sub):
        block = weight_rows(tp, sub)
        return remote(block, block, wp_send, wp_recv, {"tp": partner})

    def weight_blocks(count):
        here = all_weight_ref.at[pl.ds(0, count)]
        return remote(here, here, w_send, wp_recv, {"tp": partner})

    def weight_pairs():
        here = all_weight_ref.at[pl.ds(0, n_z)]
        return remote(here, here, wp_send, wp_recv, {"tp": partner})

    def weight_step(s, sub):
        for d in range(2):

            @pl.when(receives(d, s))
            def _():
                weight_arrival(d, s, sub).wait_recv()
                weight_pair(d, s, sub).start()

            if s + 1 < n_z - 1:

                @pl.when(sends(d, s + 1))
                def _():
                    weight_copy(d, s + 1, sub).start()

    for sub in range(2):
        for f in range(others):
            early_x(f, sub).start()
            early_y(f, sub).start()
        if sub == 0:
            loads[8].wait()
            rim_copy.start()
    loads[7].wait()
    for sub in range(SUBS):
        for d in range(2):

            @pl.when(sends(d, 0))
            def _():
                weight_copy(d, 0, sub).start()

        own_pair(sub).start()
    for k in (5, 6):
        loads[k].wait()
    lanes = lax.broadcasted_iota(jnp.int32, own_table_ref.shape, 0)
    table = jnp.zeros(own_table_ref.shape, jnp.float32)
    for k in range(routes_ref.shape[0]):
        table = table + jnp.where(
            lanes == routes_ref[k : k + 1, :], route_weight_ref[k : k + 1, :], 0.0
        )
    own_table_ref[...] = table
    for k in range(n_ep - 1):
        table_copy(k).start()
    for k in range(2, 4):
        loads[1 + k].wait()
        norm(quarters[k])
    padded_ref[: POOL_ROWS - 16] = jnp.zeros((POOL_ROWS - 16, channels), jnp.bfloat16)

    def pool():
        rim_copy.wait_recv()

        @pl.when(place == 0)
        def _():
            padded_ref[POOL_ROWS - 16 : POOL_ROWS] = jnp.zeros((16, channels), jnp.bfloat16)

        for k in (9, 10):
            loads[k].wait()
        group = channels // 4
        reach = (
            lax.broadcasted_iota(jnp.int32, (POOL_ROWS, 2 * POOL_ROWS), 0)
            + POOL_ROWS
            - lax.broadcasted_iota(jnp.int32, (POOL_ROWS, 2 * POOL_ROWS), 1)
        )
        local = lax.broadcasted_iota(jnp.int32, (POOL_ROWS, 1), 0)

        @pl.loop(0, rows // POOL_ROWS)
        def _(i):
            start = pl.multiple_of(i * POOL_ROWS, POOL_ROWS)
            here = pl.ds(start, POOL_ROWS)
            there = pl.ds(start + POOL_ROWS, POOL_ROWS)
            position = place * rows + start + local
            for which, window in enumerate(WINDOWS):
                columns = slice(which * group, (which + 1) * group)
                band = jnp.where((reach >= 0) & (reach < window), 1.0, 0.0).astype(jnp.bfloat16)
                running = jnp.dot(
                    band,
                    padded_ref[pl.ds(start, 2 * POOL_ROWS), columns],
                    preferred_element_type=jnp.float32,
                )
                count = jnp.minimum(position + 1, window).astype(jnp.float32)
                diff = running / count - padded_ref[there, columns].astype(jnp.float32)
                mixed = jnp.dot(
                    diff.astype(jnp.bfloat16),
                    pool_weight_ref[which],
                    preferred_element_type=jnp.float32,
                )
                mixed_ref[here, columns] = (mixed * pool_gain_ref[:, columns]).astype(jnp.bfloat16)

    def project(i):
        here = pl.ds(i * PROJECT_ROWS, PROJECT_ROWS)
        projected = jnp.dot(
            mixed_ref[here],
            all_weight_ref[...].reshape(channels, width),
            preferred_element_type=jnp.float32,
        )
        mix_ref[here] = rms_scale(projected, mix_gain_ref[...]).astype(jnp.bfloat16)

    def hidden(values_ref, table, first=False):
        lane = lax.broadcasted_iota(jnp.int32, (tokens, table.shape[0]), 1)
        weights = jnp.transpose(table)
        for which in range(experts):
            if first:
                for k in range(2):
                    expert_load(which, k).wait()
            weight = jnp.sum(
                jnp.where(lane == ep * experts + which, weights, 0.0), axis=1, keepdims=True
            )
            values = values_ref[...]
            gate = jnp.dot(values, gate_ref[which], preferred_element_type=jnp.float32)
            up = jnp.dot(values, up_ref[which], preferred_element_type=jnp.float32)
            hid_ref[which] = (clamped_unit(gate, up) * weight).astype(jnp.bfloat16)

    last = width // WIDE

    def partial(slot, after, lag=LAG, hook=None, at=None):
        def ended(j):
            core_copy(slot, j).wait_recv()
            for k in range(pack):
                after((j + k) // half_tiles, (j + k) % half_tiles)

        starts = [
            h * half_tiles + jj for jj in range(0, half_tiles, pack) for h in range(2)
        ]
        for i, j in enumerate(starts):
            columns = slice(j * TILE, j * TILE + WIDE)
            total = jnp.dot(
                hid_ref[0], down_ref[0, :, columns], preferred_element_type=jnp.float32
            )
            for which in range(1, experts):
                total = total + jnp.dot(
                    hid_ref[which], down_ref[which, :, columns], preferred_element_type=jnp.float32
                )
            total = total.astype(jnp.bfloat16)
            for k in range(pack):
                part_ref[j + k] = total[:, k * TILE : (k + 1) * TILE].reshape(part_ref.shape[1:])
            core_copy(slot, j).start()
            if i >= lag:
                ended(starts[i - lag])
            if hook is not None and i == (last - 1 if at is None else at):
                hook()

        def finish():
            for j in starts[len(starts) - lag :]:
                ended(j)
            core_sent(slot).wait_send()

        return finish

    def joined(k0, k1):
        return jnp.concatenate(
            [table_ref[k0, :, :piece], table_ref[k1, :, piece:]], axis=1
        )

    def core_sum(slot, h, jj):
        j = h * half_tiles + jj
        return part_ref[j, :, core].astype(jnp.float32) + core_ref[slot, j].astype(jnp.float32)

    hidden(own_ref, own_table_ref[...], first=True)
    pool()
    for e in range(experts):
        expert_load(e, 2).wait()

    def own_done(h, jj):
        acc_ref[h * half_tiles + jj] = core_sum(own, h, jj)

    steps = [(s, sub) for s in range(n_z - 1) for sub in range(SUBS)]

    def weight_steps(count):
        for step in steps[:count]:
            weight_step(*step)
        del steps[:count]


    def early_arrived(sub):
        for f in range(others):
            gathered(slot_a(f), sub, share).wait_recv()
            for g in range(others):
                pass_y(g, f, sub).start()
                pass_x(f, g, sub).start()
            for p in range(2):
                pair_copy(slot_a(f), p, sub).start()

    def early_ended():
        early_arrived(1)
        weight_steps(1)

    early_arrived(0)
    partial(own, own_done, last, early_ended)()
    tables = remote(table_ref, table_ref, table_send, table_recv, {"tp": partner})
    tables.wait_recv()

    def halves():
        return [(h, jj) for jj in range(half_tiles) for h in range(2)]

    def late_pairs():
        for f in range(others):
            gathered(slot_b(f), 0, piece).wait_recv()
            for p in range(2):
                for sub in range(2):
                    pair_copy(slot_b(f), p, sub).start()

    def diagonal_pairs(sub):
        for g in range(others):
            for f in range(others):
                gathered(slot_d(g, f), sub, share).wait_recv()
                for p in range(2):
                    pair_copy(slot_d(g, f), p, sub).start()

    def batch(slot, k0, k1, send, between=None, hook=None, at=None):
        paired(slot).wait_recv()
        hidden(x_ref.at[slot], joined(k0, k1))
        if between is not None:
            between()

        def done(h, jj):
            core_ref[slot, h * half_tiles + jj] = core_sum(slot, h, jj).astype(jnp.bfloat16)
            send(h, jj)

        return partial(slot, done, LAG, hook if others == 1 else None, at)

    def batch_a(f):
        def send(h, jj):
            first_copy(h, f, 0, jj, h, slot_a(f)).start()

        def between():
            late_x(f, 1).start()
            late_y(f, 1).start()
            if others == 1:
                diagonal_pairs(0)
                weight_steps(1)

        late_x(f, 0).start()
        late_y(f, 0).start()
        ended = functools.partial(diagonal_pairs, 1)
        batch(slot_a(f), f, (f + 1) * side - 1, send, between, ended)()

    def batch_d(i):
        g, f = (i // others, i % others) if others > 1 else (0, 0)

        def send(h, jj):
            if h == 0:
                whole_copy(0, f, g + 1, jj, slot_d(g, f)).start()
            else:
                whole_copy(1, g, f + 1, jj, slot_d(g, f)).start()

        k = (g + 1) * side + f
        between = functools.partial(weight_steps, 1) if others == 1 else None
        finish = batch(slot_d(g, f), k, k, send, between, late_pairs, 1)
        if others == 1:
            return finish
        finish()

    def batch_b(f, between=None):
        def send(h, jj):
            first_copy(h, f, 0, jj, 1 - h, slot_b(f)).start()

        batch(slot_b(f), (f + 1) * side - 1, f, send, between)()

    each(others, batch_a)
    weight_steps(2)
    if others == 1:
        finish_d = batch_d(0)
        weight_steps(1)

        def between_b():
            finish_d()
            weight_steps(1)

        batch_b(0, between_b)
    else:
        diagonal_pairs(0)
        diagonal_pairs(1)
        each(others * others, batch_d)
        weight_steps(1)
        late_pairs()
        each(others, batch_b)
    weight_steps(2)

    def second_stage(g):
        for h, jj in halves():
            for late in range(2):
                p = h if late else 1 - h
                slot, j = second_slot(h, g, p), h * half_tiles + jj
                total = core_ref[slot, j, z_rows(p)].astype(jnp.float32)
                for f in range(others):
                    if not late:
                        whole_copy(h, f, g + 1, jj, slot).wait_recv()
                    total = total + first_ref[h, f, g + 1, jj, z_rows(p)].astype(jnp.float32)
                core_ref[slot, j, z_rows(p)] = total.astype(jnp.bfloat16)
                second_copy(h, g, jj, p).start()

    each(others, second_stage)

    def plane_sum(j, h, jj):
        total = acc_ref[j]
        for f in range(others):
            whole_copy(h, f, 0, jj, own).wait_recv()
            total = total + first_ref[h, f, 0, jj].astype(jnp.float32)
        for g in range(others):
            second_arrival(h, g, jj).wait_recv()
            total = total + second_ref[h, g, jj].astype(jnp.float32)
        acc_ref[j] = total

    def z_level(level, jj):
        for h in range(2):
            j = h * half_tiles + jj
            if level == 0:
                plane_sum(j, h, jj)
            else:
                z_fold(level - 1, j)
            if level < levels:
                bit, first, count = z_part(level)
                for m in range(count):
                    zsend_ref[j, first + m] = acc_ref[j, 2 * m + 1 - bit].astype(jnp.bfloat16)
                z_copy(level, j).start()

    def z_fold(level, j):
        bit, first, count = z_part(level)
        z_copy(level, j).wait_recv()
        for m in range(count):
            acc_ref[j, m] = acc_ref[j, 2 * m + bit] + zrecv_ref[j, first + m].astype(jnp.float32)

    def straight_copy(h, k):
        return remote(
            ysend_ref.at[h, z_peer(k)],
            yrecv_ref.at[h, k],
            y_send,
            y_recv,
            {"tp": z_peer(k) * 2 + core},
        )

    straight = remote(yrecv_ref, yrecv_ref, y_send, y_recv, {"tp": partner})

    def z_straight(jj):
        for h in range(2):
            plane_sum(h * half_tiles + jj, h, jj)
            ysend_ref[h] = acc_ref[h * half_tiles + jj].astype(jnp.bfloat16)
            for k in range(n_z - 1):
                straight_copy(h, k).start()

    waves = [(level, jj) for level in range(levels) for jj in range(half_tiles - 1)]
    waves.sort(key=lambda wave: (wave[1] + 2.5 * wave[0], wave[0]))
    for i, wave in enumerate(waves[:-1]):
        z_level(*wave)
        if wave == (1, 0):
            z_straight(half_tiles - 1)
        if i in (1, 2, 3):
            weight_steps(1)
    weight_steps(len(steps))
    loads[12].wait()
    weight_pairs().wait_recv()
    project(0)
    z_level(*waves[-1])
    for i in range(1, rows // PROJECT_ROWS):
        project(i)
    loads[11].wait()

    squares = 0.0
    for jj in range(half_tiles):
        if jj < half_tiles - 1:
            z_level(levels, jj)
        else:
            straight.wait_recv()
        for h in range(2):
            j = h * half_tiles + jj
            if jj < half_tiles - 1:
                total = acc_ref[j, 0]
            else:
                total = acc_ref[j, z]
                for k in range(n_z - 1):
                    total = total + yrecv_ref[h, k].astype(jnp.float32)
                acc_ref[j, 0] = total
            squares = squares + jnp.sum(total * total, axis=-1, keepdims=True)
    scale = lax.rsqrt(squares / width + EPS)
    for j in range(tiles):
        columns = slice(j * TILE, (j + 1) * TILE)
        out_ref[:, columns] = (acc_ref[j, 0] * scale * gain_ref[:, columns]).astype(jnp.bfloat16)

    half_x = x_ref.at[:, pl.ds(0, piece)]
    remote(half_x, half_x, ag_send, rim_recv, {"tp": partner}).wait_send()
    remote(half_x, half_x, pair_send, rim_recv, {"tp": partner}).wait_send()
    tables.wait_send()
    remote(first_ref, first_ref, first_send, rim_recv, {"tp": partner}).wait_send()
    remote(second_ref, second_ref, second_send, rim_recv, {"tp": partner}).wait_send()
    halved = zsend_ref.at[pl.ds(0, 2 * (half_tiles - 1))]
    remote(halved, halved, z_send, rim_recv, {"tp": partner}).wait_send()
    straight.wait_send()
    weight_pairs().wait_send()
    for where in range(n_z):
        count = (where + 1 if where + 1 < n_z else 0) + (n_z - where if where else 0)

        @pl.when(z == where)
        def _():
            weight_blocks(count).wait_send()

    rim_copy.wait_send()


def fused(operands, n_ep, n_tp):
    expert_in, routes, _, pre_gain, gate_weight, up_weight, down_weight = operands[:7]
    pool_in, pool_weight, pool_gain, out_weight = operands[8:12]
    tokens, width = expert_in.shape
    rows, channels = pool_in.shape
    experts, _, units = gate_weight.shape
    tiles, n_z, block = width // TILE, n_tp // 2, tokens // n_tp
    side = math.isqrt(n_ep)
    others, half_tiles = side - 1, tiles // 2
    dma = pltpu.SemaphoreType.DMA
    vmem = pl.BlockSpec(memory_space=pltpu.VMEM)
    hbm = pl.BlockSpec(memory_space=pltpu.HBM)
    bf16, f32 = jnp.bfloat16, jnp.float32
    buffers = [
        (routes.shape, jnp.int32),
        (routes.shape, f32),
        (pre_gain.shape, f32),
        (pre_gain.shape, f32),
        (pool_gain.shape, f32),
        (pre_gain.shape, f32),
        ((tokens, width), bf16),
        ((tokens, width), bf16),
        ((POOL_ROWS + rows, channels), bf16),
        ((rows, channels), bf16),
        (pool_weight.shape, bf16),
        ((n_tp,) + out_weight.shape, bf16),
        ((n_ep * experts, tokens), f32),
        ((n_ep - 1, n_ep * experts, tokens), f32),
        ((n_ep - 1, tokens, width), bf16),
        (gate_weight.shape, bf16),
        (up_weight.shape, bf16),
        (down_weight.shape, bf16),
        ((experts, tokens, units), bf16),
        ((tiles, n_z, 2, block, TILE), bf16),
        ((n_ep, tiles, n_z, block, TILE), bf16),
        ((2, others, side, half_tiles, n_z, block, TILE), bf16),
        ((2, others, half_tiles, n_z, block, TILE), bf16),
        ((tiles, n_z, block, TILE), f32),
        ((tiles, n_z - 1, block, TILE), bf16),
        ((tiles, n_z - 1, block, TILE), bf16),
        ((2, n_z, block, TILE), bf16),
        ((2, n_z - 1, block, TILE), bf16),
    ]
    held = sum(math.prod(shape) * jnp.dtype(kind).itemsize for shape, kind in buffers)
    return pl.pallas_call(
        functools.partial(mixer_kernel, n_ep, n_tp),
        out_shape=(pltpu.VMEM((rows, width), bf16), pltpu.VMEM((block, width), bf16)),
        in_specs=[hbm] * len(operands),
        out_specs=(vmem, vmem),
        scratch_shapes=[pltpu.VMEM(shape, kind) for shape, kind in buffers]
        + [
            dma((len(operands) + 3 * experts,)),
            dma,
            dma,
            dma,
            dma((n_ep - 1, 2)),
            dma,
            dma((n_ep - 1,)),
            dma,
            dma((2, width // WIDE)),
            dma,
            dma((2, others, side, half_tiles)),
            dma,
            dma((2, others, half_tiles)),
            dma,
            dma((n_z.bit_length() - 1, tiles)),
            dma,
            dma,
            dma,
            dma,
            dma,
            dma((2, n_z - 1, SUBS)),
            dma,
            dma,
        ],
        compiler_params=pltpu.CompilerParams(
            collective_id=0,
            has_side_effects=True,
            vmem_limit_bytes=min(67043328, held + 10 * 2**20),
        ),
        cost_estimate=pl.CostEstimate(
            flops=6 * n_ep * tokens * experts * units * width,
            bytes_accessed=64 * 2**20,
            transcendentals=0,
        ),
        name="mixer_experts",
    )(*(pltpu.with_memory_space_constraint(operand, pltpu.HBM) for operand in operands))


def out_kernel(mix_ref, out_ref, mix_hbm, out_hbm, sems):
    copies = [
        pltpu.make_async_copy(mix_ref, mix_hbm, sems.at[0]),
        pltpu.make_async_copy(out_ref, out_hbm, sems.at[1]),
    ]
    for copy in copies:
        copy.start()
    for copy in copies:
        copy.wait()


def put_out(mix, out):
    return pl.pallas_call(
        out_kernel,
        out_shape=(
            jax.ShapeDtypeStruct(mix.shape, mix.dtype),
            jax.ShapeDtypeStruct(out.shape, out.dtype),
        ),
        in_specs=[pl.BlockSpec(memory_space=pltpu.VMEM)] * 2,
        out_specs=(pl.BlockSpec(memory_space=pltpu.HBM),) * 2,
        scratch_shapes=[pltpu.SemaphoreType.DMA((2,))],
        compiler_params=pltpu.CompilerParams(vmem_limit_bytes=2**20),
        cost_estimate=pl.CostEstimate(flops=0, bytes_accessed=2 * mix.size, transcendentals=0),
        name="put_out",
    )(
        pltpu.with_memory_space_constraint(mix, pltpu.VMEM),
        pltpu.with_memory_space_constraint(out, pltpu.VMEM),
    )


def body(
    pool_in,
    pool_weight,
    pool_gain,
    out_weight,
    mix_gain,
    expert_in,
    routes,
    route_weight,
    pre_gain,
    gate_weight,
    up_weight,
    down_weight,
    post_gain,
):
    n_ep, n_tp = lax.axis_size("ep"), lax.axis_size("tp")
    operands = (
        expert_in,
        routes.T,
        route_weight.T,
        pre_gain[None, :],
        gate_weight,
        up_weight,
        down_weight,
        post_gain[None, :],
        pool_in,
        pool_weight,
        pool_gain[None, :],
        out_weight,
        mix_gain[None, :],
    )
    return put_out(*fused(operands, n_ep, n_tp))


def solution(mesh):
    return jax.shard_map(
        body,
        mesh=mesh,
        in_specs=(
            P(("ep", "tp"), None),
            P(),
            P(),
            P("tp", None),
            P(),
            P("ep", None),
            P("ep", None),
            P("ep", None),
            P(),
            P("ep", None, "tp"),
            P("ep", None, "tp"),
            P("ep", "tp", None),
            P(),
        ),
        out_specs=(P(("ep", "tp"), None), P(("ep", "tp"), None)),
        check_vma=False,
    )
```

time: 60.8 us -> 55.1 us (0.906)
  Pallas kernels: 58 us -> 54.1 us
  local copies, waits for them, and re-layouts: 1.98 us -> 0 us
    pallas_call x1, Pallas kernels: 58 us -> 52.8 us  [fused(): pl.pallas_call(functools.partial(mixer_kernel, n_ep, n_tp), out_shape=(pl...]
    unnamed x2 -> x0, local copies, waits for them, and re-layouts: 1.98 us -> none
    pallas_call x0 -> x1, Pallas kernels: none -> 1.36 us  [put_out(): pl.pallas_call(out_kernel, out_shape=(jax.ShapeDtypeStruct(mix.shape, mix...]
where the time goes in v2:
time: 55.1 us; the launch traced here: 54.9 us
  Pallas kernels  54.1 us (98%)
  between operations  0.8 us (1%)
    pallas_call x1, Pallas kernels, fused(): pl.pallas_call(functools.partial(mixer_kernel, n_ep, n_tp), out_shape=(pl...  52.8 us
    pallas_call x1, Pallas kernels, put_out(): pl.pallas_call(out_kernel, out_shape=(jax.ShapeDtypeStruct(mix.shape, mix...  1.36 us

profile of v2, /device:TPU:0, one launch (start us, length us, event | category | flops | bytes accessed | tf_op | source)
XLA Modules:
  0.0 54.9 jit_solution(8299316654607393918)
XLA Ops:
  0.6 52.8 %mixer_experts.1 = (bf16[512,2048]{1,0:T(8,128)(2,1)S(1)}, bf16[32,2048]{1,0:T(8,128)(2,1)S(1)}) custom-call(bf16[256,2048]{1,0:T(8,128)(2,1)} %expert_hbm.1, s32[4,256]{1,0:T(4,128)} %bitcast.9, f32[4,256]{1,0:T(4,128)} %bitcast.10, f32[1,2048]{1,0:T(1,128)} %bitcast.6, bf16[2,2048,512]{2,1,0:T(8,128)(2,1)} %gate_hbm.1, bf16[2,2048,512]{2,1,0:T(8,128)(2,1)} %up_hbm.1, ...), custom_call_target="tpu_custom_call" | custom-call | flops 12884901888 | bytes 67108864 | tf_op jit(solution)/shard_map/mixer_experts/pallas_call | solution.py:854
  53.4 1.4 %put_out.1 = (bf16[512,2048]{1,0:T(8,128)(2,1)}, bf16[32,2048]{1,0:T(8,128)(2,1)}) custom-call(bf16[512,2048]{1,0:T(8,128)(2,1)S(1)} %get-tuple-element.4.mix_ref, bf16[32,2048]{1,0:T(8,128)(2,1)S(1)} %get-tuple-element.5.out_ref), custom_call_target="tpu_custom_call" | custom-call | bytes 2097152 | tf_op jit(solution)/shard_map/put_out/pallas_call | solution.py:911

commit v3 on v2

--- a/solution.py
+++ b/solution.py
@@ -91,12 +91,11 @@
     part_ref,
     core_ref,
     first_ref,
+    send_ref,
     second_ref,
     acc_ref,
     zsend_ref,
     zrecv_ref,
-    ysend_ref,
-    yrecv_ref,
     load_sem,
     table_send,
     table_recv,
@@ -112,8 +111,6 @@
     second_recv,
     z_send,
     z_recv,
-    y_send,
-    y_recv,
     rim_send,
     rim_recv,
     w_send,
@@ -244,18 +241,18 @@
         size = share // 2
         return pl.ds(pl.multiple_of(p * piece + core * share + sub * size, size), size)
 
-    def gather_copy(source, slot, p, sub, device, together=False):
+    def gather_copy(source, slot, p, sub, device):
         here = half_rows(p, sub)
         return remote(
             source.at[here],
             x_ref.at[slot, here],
             ag_send,
-            ag_recv.at[slot, 0 if together else sub],
+            ag_recv.at[slot, sub],
             device,
         )
 
-    def gathered(slot, sub, count):
-        here = x_ref.at[slot, pl.ds(0, count)]
+    def gathered(slot, sub):
+        here = x_ref.at[slot, pl.ds(0, share)]
         return remote(here, here, ag_send, ag_recv.at[slot, sub], {"tp": partner})
 
     def early_x(f, sub):
@@ -265,10 +262,10 @@
         return gather_copy(own_ref, slot_a(f), 1, sub, y_peer(f))
 
     def late_x(f, sub):
-        return gather_copy(own_ref, slot_b(f), 1, sub, x_peer(f), True)
+        return gather_copy(own_ref, slot_b(f), 1, sub, x_peer(f))
 
     def late_y(f, sub):
-        return gather_copy(own_ref, slot_b(f), 0, sub, y_peer(f), True)
+        return gather_copy(own_ref, slot_b(f), 0, sub, y_peer(f))
 
     def pass_y(g, f, sub):
         return gather_copy(x_ref.at[slot_a(f)], slot_d(g, f), 0, sub, y_peer(g))
@@ -310,31 +307,38 @@
     def z_rows(p):
         return pl.ds(p * half_z, half_z)
 
-    def first_copy(h, f, g, jj, p, slot):
+    def packed(jj):
+        return pl.ds(jj // pack * pack, pack)
+
+    def first_copy(h, f, jj, p, slot):
         return remote(
-            core_ref.at[slot, h * half_tiles + jj, z_rows(p)],
-            first_ref.at[h, f, g, jj, z_rows(p)],
+            core_ref.at[slot, pl.ds(h * half_tiles + jj, pack), z_rows(p)],
+            first_ref.at[h, f, 0, pl.ds(jj, pack), z_rows(p)],
             first_send,
-            first_recv.at[h, f, g, jj],
+            first_recv.at[h, f, 0, jj // pack],
             x_peer(f) if h == 0 else y_peer(f),
         )
 
     def whole_copy(h, f, g, jj, slot):
         return remote(
-            core_ref.at[slot, h * half_tiles + jj],
-            first_ref.at[h, f, g, jj],
+            core_ref.at[slot, pl.ds(h * half_tiles + jj, pack)],
+            first_ref.at[h, f, g, pl.ds(jj, pack)],
             first_send,
-            first_recv.at[h, f, g, jj],
+            first_recv.at[h, f, g, jj // pack],
             x_peer(f) if h == 0 else y_peer(f),
         )
+
+    def first_arrival(h, f, g, jj):
+        here = first_ref.at[h, f, g, packed(jj)]
+        return remote(here, here, first_send, first_recv.at[h, f, g, jj // pack], {"tp": partner})
 
     def second_slot(h, g, p):
         return slot_a(g) if h != p else slot_b(g)
 
-    def second_copy(h, g, jj, p):
+    def second_copy(h, g, jj):
         return remote(
-            core_ref.at[second_slot(h, g, p), h * half_tiles + jj, z_rows(p)],
-            second_ref.at[h, g, jj, z_rows(p)],
+            send_ref.at[h, g, jj],
+            second_ref.at[h, g, jj],
             second_send,
             second_recv.at[h, g, jj],
             y_peer(g) if h == 0 else x_peer(g),
@@ -526,8 +530,7 @@
     def partial(slot, after, lag=LAG, hook=None, at=None):
         def ended(j):
             core_copy(slot, j).wait_recv()
-            for k in range(pack):
-                after((j + k) // half_tiles, (j + k) % half_tiles)
+            after(j)
 
         starts = [
             h * half_tiles + jj for jj in range(0, half_tiles, pack) for h in range(2)
@@ -562,8 +565,7 @@
             [table_ref[k0, :, :piece], table_ref[k1, :, piece:]], axis=1
         )
 
-    def core_sum(slot, h, jj):
-        j = h * half_tiles + jj
+    def core_sum(slot, j):
         return part_ref[j, :, core].astype(jnp.float32) + core_ref[slot, j].astype(jnp.float32)
 
     hidden(own_ref, own_table_ref[...], first=True)
@@ -571,8 +573,9 @@
     for e in range(experts):
         expert_load(e, 2).wait()
 
-    def own_done(h, jj):
-        acc_ref[h * half_tiles + jj] = core_sum(own, h, jj)
+    def own_done(j):
+        for k in range(pack):
+            acc_ref[j + k] = core_sum(own, j + k)
 
     steps = [(s, sub) for s in range(n_z - 1) for sub in range(SUBS)]
 
@@ -584,7 +587,7 @@
 
     def early_arrived(sub):
         for f in range(others):
-            gathered(slot_a(f), sub, share).wait_recv()
+            gathered(slot_a(f), sub).wait_recv()
             for g in range(others):
                 pass_y(g, f, sub).start()
                 pass_x(f, g, sub).start()
@@ -603,17 +606,16 @@
     def halves():
         return [(h, jj) for jj in range(half_tiles) for h in range(2)]
 
-    def late_pairs():
+    def late_pairs(sub):
         for f in range(others):
-            gathered(slot_b(f), 0, piece).wait_recv()
+            gathered(slot_b(f), sub).wait_recv()
             for p in range(2):
-                for sub in range(2):
-                    pair_copy(slot_b(f), p, sub).start()
+                pair_copy(slot_b(f), p, sub).start()
 
     def diagonal_pairs(sub):
         for g in range(others):
             for f in range(others):
-                gathered(slot_d(g, f), sub, share).wait_recv()
+                gathered(slot_d(g, f), sub).wait_recv()
                 for p in range(2):
                     pair_copy(slot_d(g, f), p, sub).start()
 
@@ -623,15 +625,16 @@
         if between is not None:
             between()
 
-        def done(h, jj):
-            core_ref[slot, h * half_tiles + jj] = core_sum(slot, h, jj).astype(jnp.bfloat16)
-            send(h, jj)
+        def done(j):
+            for k in range(pack):
+                core_ref[slot, j + k] = core_sum(slot, j + k).astype(jnp.bfloat16)
+            send(j // half_tiles, j % half_tiles)
 
         return partial(slot, done, LAG, hook if others == 1 else None, at)
 
     def batch_a(f):
         def send(h, jj):
-            first_copy(h, f, 0, jj, h, slot_a(f)).start()
+            first_copy(h, f, jj, h, slot_a(f)).start()
 
         def between():
             late_x(f, 1).start()
@@ -655,15 +658,20 @@
                 whole_copy(1, g, f + 1, jj, slot_d(g, f)).start()
 
         k = (g + 1) * side + f
-        between = functools.partial(weight_steps, 1) if others == 1 else None
-        finish = batch(slot_d(g, f), k, k, send, between, late_pairs, 1)
+
+        def between():
+            late_pairs(0)
+            weight_steps(1)
+
+        ended = functools.partial(late_pairs, 1)
+        finish = batch(slot_d(g, f), k, k, send, between if others == 1 else None, ended)
         if others == 1:
             return finish
         finish()
 
     def batch_b(f, between=None):
         def send(h, jj):
-            first_copy(h, f, 0, jj, 1 - h, slot_b(f)).start()
+            first_copy(h, f, jj, 1 - h, slot_b(f)).start()
 
         batch(slot_b(f), (f + 1) * side - 1, f, send, between)()
 
@@ -683,29 +691,32 @@
         diagonal_pairs(1)
         each(others * others, batch_d)
         weight_steps(1)
-        late_pairs()
+        late_pairs(0)
+        late_pairs(1)
         each(others, batch_b)
     weight_steps(2)
 
     def second_stage(g):
         for h, jj in halves():
-            for late in range(2):
-                p = h if late else 1 - h
-                slot, j = second_slot(h, g, p), h * half_tiles + jj
-                total = core_ref[slot, j, z_rows(p)].astype(jnp.float32)
+            for f in range(others):
+                if jj % pack == 0:
+                    first_arrival(h, f, g + 1, jj).wait_recv()
+            for p in range(2):
+                total = core_ref[second_slot(h, g, p), h * half_tiles + jj, z_rows(p)].astype(
+                    jnp.float32
+                )
                 for f in range(others):
-                    if not late:
-                        whole_copy(h, f, g + 1, jj, slot).wait_recv()
                     total = total + first_ref[h, f, g + 1, jj, z_rows(p)].astype(jnp.float32)
-                core_ref[slot, j, z_rows(p)] = total.astype(jnp.bfloat16)
-                second_copy(h, g, jj, p).start()
+                send_ref[h, g, jj, z_rows(p)] = total.astype(jnp.bfloat16)
+            second_copy(h, g, jj).start()
 
     each(others, second_stage)
 
     def plane_sum(j, h, jj):
         total = acc_ref[j]
         for f in range(others):
-            whole_copy(h, f, 0, jj, own).wait_recv()
+            if jj % pack == 0:
+                first_arrival(h, f, 0, jj).wait_recv()
             total = total + first_ref[h, f, 0, jj].astype(jnp.float32)
         for g in range(others):
             second_arrival(h, g, jj).wait_recv()
@@ -717,7 +728,7 @@
             j = h * half_tiles + jj
             if level == 0:
                 plane_sum(j, h, jj)
-            else:
+            if level > 0:
                 z_fold(level - 1, j)
             if level < levels:
                 bit, first, count = z_part(level)
@@ -731,36 +742,17 @@
         for m in range(count):
             acc_ref[j, m] = acc_ref[j, 2 * m + bit] + zrecv_ref[j, first + m].astype(jnp.float32)
 
-    def straight_copy(h, k):
-        return remote(
-            ysend_ref.at[h, z_peer(k)],
-            yrecv_ref.at[h, k],
-            y_send,
-            y_recv,
-            {"tp": z_peer(k) * 2 + core},
-        )
-
-    straight = remote(yrecv_ref, yrecv_ref, y_send, y_recv, {"tp": partner})
-
-    def z_straight(jj):
-        for h in range(2):
-            plane_sum(h * half_tiles + jj, h, jj)
-            ysend_ref[h] = acc_ref[h * half_tiles + jj].astype(jnp.bfloat16)
-            for k in range(n_z - 1):
-                straight_copy(h, k).start()
-
-    waves = [(level, jj) for level in range(levels) for jj in range(half_tiles - 1)]
+    waves = [(level, jj) for level in range(levels) for jj in range(half_tiles)]
     waves.sort(key=lambda wave: (wave[1] + 2.5 * wave[0], wave[0]))
     for i, wave in enumerate(waves[:-1]):
         z_level(*wave)
-        if wave == (1, 0):
-            z_straight(half_tiles - 1)
-        if i in (1, 2, 3):
+        if i in (1, 3):
             weight_steps(1)
-    weight_steps(len(steps))
-    loads[12].wait()
-    weight_pairs().wait_recv()
-    project(0)
+        if wave == (1, 1):
+            weight_steps(len(steps))
+            loads[12].wait()
+            weight_pairs().wait_recv()
+            project(0)
     z_level(*waves[-1])
     for i in range(1, rows // PROJECT_ROWS):
         project(i)
@@ -768,19 +760,9 @@
 
     squares = 0.0
     for jj in range(half_tiles):
-        if jj < half_tiles - 1:
-            z_level(levels, jj)
-        else:
-            straight.wait_recv()
+        z_level(levels, jj)
         for h in range(2):
-            j = h * half_tiles + jj
-            if jj < half_tiles - 1:
-                total = acc_ref[j, 0]
-            else:
-                total = acc_ref[j, z]
-                for k in range(n_z - 1):
-                    total = total + yrecv_ref[h, k].astype(jnp.float32)
-                acc_ref[j, 0] = total
+            total = acc_ref[h * half_tiles + jj, 0]
             squares = squares + jnp.sum(total * total, axis=-1, keepdims=True)
     scale = lax.rsqrt(squares / width + EPS)
     for j in range(tiles):
@@ -793,9 +775,7 @@
     tables.wait_send()
     remote(first_ref, first_ref, first_send, rim_recv, {"tp": partner}).wait_send()
     remote(second_ref, second_ref, second_send, rim_recv, {"tp": partner}).wait_send()
-    halved = zsend_ref.at[pl.ds(0, 2 * (half_tiles - 1))]
-    remote(halved, halved, z_send, rim_recv, {"tp": partner}).wait_send()
-    straight.wait_send()
+    remote(zsend_ref, zsend_ref, z_send, rim_recv, {"tp": partner}).wait_send()
     weight_pairs().wait_send()
     for where in range(n_z):
         count = (where + 1 if where + 1 < n_z else 0) + (n_z - where if where else 0)
@@ -844,11 +824,10 @@
         ((n_ep, tiles, n_z, block, TILE), bf16),
         ((2, others, side, half_tiles, n_z, block, TILE), bf16),
         ((2, others, half_tiles, n_z, block, TILE), bf16),
+        ((2, others, half_tiles, n_z, block, TILE), bf16),
         ((tiles, n_z, block, TILE), f32),
         ((tiles, n_z - 1, block, TILE), bf16),
         ((tiles, n_z - 1, block, TILE), bf16),
-        ((2, n_z, block, TILE), bf16),
-        ((2, n_z - 1, block, TILE), bf16),
     ]
     held = sum(math.prod(shape) * jnp.dtype(kind).itemsize for shape, kind in buffers)
     return pl.pallas_call(
@@ -868,13 +847,11 @@
             dma,
             dma((2, width // WIDE)),
             dma,
-            dma((2, others, side, half_tiles)),
+            dma((2, others, side, width // WIDE // 2)),
             dma,
             dma((2, others, half_tiles)),
             dma,
             dma((n_z.bit_length() - 1, tiles)),
-            dma,
-            dma,
             dma,
             dma,
             dma,

time: 55.1 us -> 54.7 us (level)
  no operation moved by 1% of the time
where the time goes in v3:
time: 54.7 us; the launch traced here: 54.5 us
  Pallas kernels  53.7 us (98%)
  between operations  0.8 us (1%)
    pallas_call x1, Pallas kernels, fused(): pl.pallas_call(functools.partial(mixer_kernel, n_ep, n_tp), out_shape=(pl...  52.4 us
    pallas_call x1, Pallas kernels, put_out(): pl.pallas_call(out_kernel, out_shape=(jax.ShapeDtypeStruct(mix.shape, mix...  1.36 us

profile of v3, /device:TPU:0, one launch (start us, length us, event | category | flops | bytes accessed | tf_op | source)
XLA Modules:
  0.0 54.5 jit_solution(17532670114162362896)
XLA Ops:
  0.6 52.4 %mixer_experts.1 = (bf16[512,2048]{1,0:T(8,128)(2,1)S(1)}, bf16[32,2048]{1,0:T(8,128)(2,1)S(1)}) custom-call(bf16[256,2048]{1,0:T(8,128)(2,1)} %expert_hbm.1, s32[4,256]{1,0:T(4,128)} %bitcast.9, f32[4,256]{1,0:T(4,128)} %bitcast.10, f32[1,2048]{1,0:T(1,128)} %bitcast.6, bf16[2,2048,512]{2,1,0:T(8,128)(2,1)} %gate_hbm.1, bf16[2,2048,512]{2,1,0:T(8,128)(2,1)} %up_hbm.1, ...), custom_call_target="tpu_custom_call" | custom-call | flops 12884901888 | bytes 67108864 | tf_op jit(solution)/shard_map/mixer_experts/pallas_call | solution.py:833
  53.0 1.4 %put_out.1 = (bf16[512,2048]{1,0:T(8,128)(2,1)}, bf16[32,2048]{1,0:T(8,128)(2,1)}) custom-call(bf16[512,2048]{1,0:T(8,128)(2,1)S(1)} %get-tuple-element.4.mix_ref, bf16[32,2048]{1,0:T(8,128)(2,1)S(1)} %get-tuple-element.5.out_ref), custom_call_target="tpu_custom_call" | custom-call | bytes 2097152 | tf_op jit(solution)/shard_map/put_out/pallas_call | solution.py:888
